TPU v7x, 512 devices: a 8x2x16 block of a 8x16x16 slice. The times are simulated.
512 devices in a mesh: grp: 2 (over y), sp: 16 (over z), tp: 16 (over x, core).
Axes of the slice: x: 8, y: 2, z: 16, core: 2. Of those that a mesh axis runs over, the one named last changes fastest.
The devices are a block of a 8x16x16 slice.
Arguments:
- target: bfloat16 [4096, 2048], P(('grp', 'sp', 'tp')), parts along dimension 0, may hold values from -60 to 60
- source: bfloat16 [32768, 2048], P(('grp', 'sp', 'tp')), parts along dimension 0, may hold values from -120 to 120
- w_query: bfloat16 [2, 2048, 2048], P(None, None, 'tp'), may hold values from -0.176776695 to 0.176776695
- w_key: bfloat16 [2, 2048, 2048], P(None, None, 'tp'), may hold values from -0.176776695 to 0.176776695
- w_value: bfloat16 [2, 2048, 2048], P(None, None, 'tp'), may hold values from -0.125 to 0.125
- w_out: bfloat16 [2, 2048, 2048], P(None, 'tp'), may hold values from -0.125 to 0.125
- gains: float32 [2, 2, 2048], replicated, may hold values from 0.1 to 1.9
Outputs:
- mixed: bfloat16 [4096, 2048], P(('grp', 'sp', 'tp')), parts along dimension 0
There are 2 independent parts, one for each index of `grp`. A program takes and returns all parts, laid end to end along the dimension named above; an argument that names none is the same for every part. Nothing has to cross between parts.
All inputs are finite; a program needn't handle non-finite values.
Results may differ from a plain program's by a relative error of at most 0.025.
Values may be sent and summed in bfloat16 or wider, within the bound.
No kernel may reach another device: no remote copies, remote signals or barrier semaphores. Data moves between devices by JAX's collectives and lax.ppermute only.
A program may use at most 128 MiB of HBM per device.

v0:
```python
import jax
import jax.numpy as jnp
from jax import lax
from jax.sharding import Mesh
from jax.sharding import PartitionSpec as P

HEAD = 128
TP = ("tp_0", "tp_1")
GRP_SP_TP = ("grp", "sp", "tp_0", "tp_1")


EPS = 1e-06


def in_order(parts, dim):
    dims = list(parts.shape[1:])
    dims[dim] *= parts.shape[0]
    return jnp.moveaxis(parts, 0, dim).reshape(dims)


def stacked_from(x, axes, order):
    parts = x
    for k in order:
        parts = lax.all_gather(parts, axes[k])
    done = order[::-1]
    back = [done.index(k) for k in range(len(axes))]
    parts = parts.transpose(*back, *range(len(axes), parts.ndim))
    return parts.reshape(-1, *x.shape)


def whole_of(x, axes, order, dim):
    return in_order(stacked_from(x, axes, order), dim)


def sent_together(arrays, axis, dim, along):
    both = jnp.concatenate(arrays, axis=along)
    result, at, gathered = (lax.all_gather(both, axis, axis=dim, tiled=True), 0, [])
    for a in arrays:
        gathered.append(lax.slice_in_dim(result, at, at + a.shape[along], axis=along))
        at += a.shape[along]
    return tuple(gathered)


def split_up(x, dim, peers):
    dims = x.shape
    parts = x.reshape(*dims[:dim], peers, dims[dim] // peers, *dims[dim + 1 :])
    return jnp.moveaxis(parts, dim, 0)


def sum_at_owner(x, axis, dim):
    peers = lax.axis_size(axis)
    parts = lax.all_to_all(split_up(x, dim, peers), axis, 0, 0, tiled=True)
    return jnp.sum(parts.astype(jnp.float32), axis=0)


def normalize(row_block, gain_row):
    return (
        row_block
        * lax.rsqrt(jnp.mean(row_block * row_block, axis=-1, keepdims=True) + EPS)
        * gain_row
    )


def split_heads(row_block):
    return row_block.reshape(row_block.shape[0], row_block.shape[1] // HEAD, HEAD)


def body(target, source, w_query, w_key, w_value, w_out, gains):
    local_width = w_query.shape[2]
    heads_here = local_width // HEAD
    score_scale = HEAD ** (-0.5)
    depth = w_query.shape[0]
    project_shard_part = lax.all_gather(source, TP, axis=0, tiled=True)
    layer_parts = [
        jnp.stack(
            [
                jnp.dot(project_shard_part, w_key[level], preferred_element_type=jnp.float32),
                jnp.dot(project_shard_part, w_value[level], preferred_element_type=jnp.float32),
            ]
        )
        for level in range(depth)
    ]
    projected_source = jnp.stack(layer_parts).astype(jnp.bfloat16)
    stream = target.astype(jnp.float32)
    for layer_index in range(depth):
        normed = normalize(stream, gains[layer_index, 0]).astype(jnp.bfloat16)
        query_weight = w_query[layer_index]
        queries = jnp.dot(
            whole_of(normed, ("tp_0", "tp_1"), (0, 1), 0),
            query_weight,
            preferred_element_type=jnp.float32,
        ).astype(jnp.bfloat16)
        row_count = queries.shape[0]
        keys_here = projected_source[layer_index, 0]
        values_here = projected_source[layer_index, 1]
        query_heads = split_heads(queries)
        shard_part = sent_together((keys_here, values_here), "sp", 0, 1)
        row_peak = jnp.full((heads_here, row_count), -1e30, jnp.float32)
        key_heads = split_heads(shard_part[0])
        value_heads = split_heads(shard_part[1])
        scores = (
            jnp.einsum("qhd,khd->hqk", query_heads, key_heads, preferred_element_type=jnp.float32)
            * score_scale
        )
        new_peak = jnp.maximum(row_peak, jnp.max(scores, axis=2))
        weights = jnp.exp(scores - new_peak[:, :, None])
        row_total = jnp.sum(weights, axis=2)
        summed = jnp.einsum(
            "hqk,khd->hqd",
            weights.astype(jnp.bfloat16),
            value_heads,
            preferred_element_type=jnp.float32,
        )
        row_peak, row_total, summed = (new_peak, row_total, summed)
        heads_out = summed / row_total[:, :, None]
        attended = (
            jnp.transpose(heads_out, (1, 0, 2)).reshape(row_count, local_width).astype(jnp.bfloat16)
        )
        out_weight = w_out[layer_index]
        projected = sum_at_owner(
            jnp.dot(attended, out_weight, preferred_element_type=jnp.float32).astype(jnp.bfloat16),
            TP,
            0,
        )
        stream = stream + normalize(projected, gains[layer_index, 1])
    return stream.astype(jnp.bfloat16)


def solution(mesh):
    split = Mesh(
        mesh.devices.reshape(mesh.shape["grp"], mesh.shape["sp"], 8, 2),
        ("grp", "sp", "tp_0", "tp_1"),
    )
    placed = (
        P(GRP_SP_TP, None),
        P(GRP_SP_TP, None),
        P(None, None, TP),
        P(None, None, TP),
        P(None, None, TP),
        P(None, TP, None),
        P(),
    )
    return jax.shard_map(
        body, mesh=split, in_specs=placed, out_specs=P(GRP_SP_TP, None), check_vma=False
    )
```

profile of v0, /device:TPU:65, one launch (start us, length us, event | category | flops | bytes accessed | tf_op | source)
XLA Modules:
  0.0 365.9 jit_solution(10650329462650321292)
XLA Ops:
  6.6 0.7 all-gather.8.cloned.1.call-update
  7.4 85.2 %all-gather.8.cloned.1.call-done = bf16[1024,2048]{1,0:T(8,128)(2,1)} async-done(((bf16[64,2048]{1,0:T(8,128)(2,1)}), bf16[1024,2048]{1,0:T(8,128)(2,1)}) %all-gather.8.cloned.1.call-update) | async-done | bytes 4194320 | tf_op jit(solution)/shard_map/all_gather | solution.py:73
  92.6 3.8 %fusion.16 = bf16[1,1024,128]{1,2,0:T(8,128)(2,1)S(1)} fusion(bf16[1024,2048]{1,0:T(8,128)(2,1)} %all-gather.8.cloned.1.call-done, bf16[2,2048,128]{2,1,0:T(8,128)(2,1)} %param.10), kind=kOutput, calls=%fused_computation.24 | convolution fusion | flops 537001984 | bytes 4980736 | tf_op jit(solution)/shard_map/dot_general | solution.py:77
  96.4 3.8 %fusion.17 = bf16[1,1024,128]{1,2,0:T(8,128)(2,1)S(1)} fusion(bf16[1024,2048]{1,0:T(8,128)(2,1)} %all-gather.8.cloned.1.call-done, bf16[2,2048,128]{2,1,0:T(8,128)(2,1)} %param.11), kind=kOutput, calls=%fused_computation.25 | convolution fusion | flops 537001984 | bytes 4980736 | tf_op jit(solution)/shard_map/dot_general | solution.py:78
  100.4 0.8 pad_maximum_fusion
  101.3 0.1 all-gather.12.cloned.1.call-start
  101.4 3.8 %fusion.18 = bf16[1,1024,128]{1,2,0:T(8,128)(2,1)S(1)} fusion(bf16[1024,2048]{1,0:T(8,128)(2,1)} %all-gather.8.cloned.1.call-done, bf16[2,2048,128]{2,1,0:T(8,128)(2,1)S(1)} %copy-done), kind=kOutput, calls=%fused_computation.26 | convolution fusion | flops 537001984 | bytes 4980736 | tf_op jit(solution)/shard_map/dot_general | solution.py:77
  105.2 3.7 %fusion.19 = bf16[1,1024,128]{1,2,0:T(8,128)(2,1)S(1)} fusion(bf16[1024,2048]{1,0:T(8,128)(2,1)} %all-gather.8.cloned.1.call-done, bf16[2,2048,128]{2,1,0:T(8,128)(2,1)S(1)} %copy-done.1), kind=kOutput, calls=%fused_computation.27 | convolution fusion | flops 537001984 | bytes 4980736 | tf_op jit(solution)/shard_map/dot_general | solution.py:78
  109.0 0.9 pad_maximum_fusion.1
  109.9 0.1 fusion.68
  110.1 0.1 fusion.70
  110.2 19.9 %all-gather = bf16[64,2048]{1,0:T(8,128)(2,1)S(1)} all-gather(bf16[8,2048]{1,0:T(8,128)(2,1)S(1)} %fusion.70), channel_id=2, replica_groups=mesh['grp'=2,'sp'=16,'tp_0'=8,'tp_1'=2] {'tp_0'}, dimensions={0}, use_global_device_ids=true | all-gather | bytes 294912 | tf_op jit(solution)/shard_map/all_gather | solution.py:24
  130.0 7.1 %all-gather.1 = bf16[16,8,2048]{2,1,0:T(8,128)(2,1)S(1)} all-gather(bf16[8,8,2048]{2,1,0:T(8,128)(2,1)S(1)} %bitcast.78), channel_id=3, replica_groups=mesh['grp'=2,'sp'=16,'tp_0'=8,'tp_1'=2] {'tp_1'}, dimensions={0}, use_global_device_ids=true | all-gather | bytes 786432 | tf_op jit(solution)/shard_map/all_gather | solution.py:24
  137.1 71.2 %all-gather.10.cloned.1.call-done = bf16[16384,256]{0,1:T(8,128)(2,1)} async-done(((bf16[1024,256]{0,1:T(8,128)(2,1)}), bf16[16384,256]{0,1:T(8,128)(2,1)}) %all-gather.10.cloned.1.call-update) | async-done | bytes 8388624 | tf_op jit(solution)/shard_map/all_gather | solution.py:37
  208.4 7.0 %fusion.74 = (f32[128]{0:T(128)S(1)}, f32[128,16384]{1,0:T(8,128)}) fusion(bf16[16384,256]{0,1:T(8,128)(2,1)} %all-gather.10.cloned.1.call-done, bf16[128,2048]{1,0:T(8,128)(2,1)S(1)} %bitcast.76, bf16[2,2048,128]{2,1,0:T(8,128)(2,1)S(1)} %copy-done.3), kind=kOutput, calls=%fused_computation.80 | convolution fusion | flops 608190336 | bytes 13632000 | tf_op jit(solution)/shard_map/qhd,khd->hqk/dot_general | solution.py:102
  215.3 4.7 %fusion = f32[128]{0:T(128)S(1)} fusion(f32[128,16384]{1,0:T(8,128)} %get-tuple-element.14, f32[128]{0:T(128)S(1)} %broadcast_maximum_fusion.1), kind=kLoop, calls=%fused_computation.4 | loop fusion | flops 4194176 | bytes 8389632 | tf_op jit(solution)/shard_map/reduce_sum | solution.py:107
  220.0 6.4 %fusion.14 = bf16[16,8,2048]{2,1,0:T(8,128)(2,1)S(1)} fusion(bf16[16384,256]{0,1:T(8,128)(2,1)} %all-gather.10.cloned.1.call-done, f32[128,16384]{1,0:T(8,128)} %get-tuple-element.14, f32[128]{0:T(128)S(1)} %broadcast_maximum_fusion.1, bf16[2,128,2048]{2,1,0:T(8,128)(2,1)S(1)} %copy-done.2, f32[128]{0:T(128)S(1)} %fusion), kind=kOutput, calls=%fused_computation.18 | convolution fusion | flops 608468992 | bytes 13632512 | tf_op jit(solution)/shard_map/dot_general | solution.py:121
  226.4 24.5 %all_to_all.10 = bf16[16,8,2048]{2,1,0:T(8,128)(2,1)S(1)} all-to-all(bf16[16,8,2048]{2,1,0:T(8,128)(2,1)S(1)} %fusion.14), channel_id=1, replica_groups=mesh['grp'=2,'sp'=16,'tp_0'=8,'tp_1'=2] {'tp_0','tp_1'}, dimensions={0} | all-to-all | bytes 1048576 | tf_op jit(solution)/shard_map/all_to_all | solution.py:52
  251.0 0.1 convert_reduce_fusion.1
  251.0 0.1 multiply_reduce_fusion.2
  251.2 0.2 multiply_reduce_fusion.1
  251.4 0.1 multiply_convert_fusion
  251.5 21.5 %all-gather.2 = bf16[64,2048]{1,0:T(8,128)(2,1)S(1)} all-gather(bf16[8,2048]{1,0:T(8,128)(2,1)S(1)} %multiply_convert_fusion), channel_id=4, replica_groups=mesh['grp'=2,'sp'=16,'tp_0'=8,'tp_1'=2] {'tp_0'}, dimensions={0}, use_global_device_ids=true | all-gather | bytes 294912 | tf_op jit(solution)/shard_map/all_gather | solution.py:24
  272.9 4.2 %all-gather.3 = bf16[16,8,2048]{2,1,0:T(8,128)(2,1)S(1)} all-gather(bf16[8,8,2048]{2,1,0:T(8,128)(2,1)S(1)} %bitcast.79), channel_id=5, replica_groups=mesh['grp'=2,'sp'=16,'tp_0'=8,'tp_1'=2] {'tp_1'}, dimensions={0}, use_global_device_ids=true | all-gather | bytes 786432 | tf_op jit(solution)/shard_map/all_gather | solution.py:24
  277.2 38.7 %all-gather.12.cloned.1.call-done = bf16[16384,256]{0,1:T(8,128)(2,1)} async-done(((bf16[1024,256]{0,1:T(8,128)(2,1)}), bf16[16384,256]{0,1:T(8,128)(2,1)}) %all-gather.12.cloned.1.call-update) | async-done | bytes 8388624 | tf_op jit(solution)/shard_map/all_gather | solution.py:37
  315.9 6.9 %fusion.77 = (f32[128]{0:T(128)S(1)}, f32[128,16384]{1,0:T(8,128)}) fusion(bf16[16384,256]{0,1:T(8,128)(2,1)} %all-gather.12.cloned.1.call-done, bf16[128,2048]{1,0:T(8,128)(2,1)S(1)} %bitcast.77, bf16[2,2048,128]{2,1,0:T(8,128)(2,1)S(1)} %copy-done.3), kind=kOutput, calls=%fused_computation.81 | convolution fusion | flops 608190336 | bytes 13632000 | tf_op jit(solution)/shard_map/qhd,khd->hqk/dot_general | solution.py:102
  322.8 4.7 %fusion.2 = f32[128]{0:T(128)S(1)} fusion(f32[128,16384]{1,0:T(8,128)} %get-tuple-element.16, f32[128]{0:T(128)S(1)} %broadcast_maximum_fusion), kind=kLoop, calls=%fused_computation.6 | loop fusion | flops 4194176 | bytes 8389632 | tf_op jit(solution)/shard_map/reduce_sum | solution.py:107
  327.5 6.4 %fusion.15 = bf16[16,8,2048]{2,1,0:T(8,128)(2,1)S(1)} fusion(bf16[16384,256]{0,1:T(8,128)(2,1)} %all-gather.12.cloned.1.call-done, f32[128,16384]{1,0:T(8,128)} %get-tuple-element.16, f32[128]{0:T(128)S(1)} %broadcast_maximum_fusion, bf16[2,128,2048]{2,1,0:T(8,128)(2,1)S(1)} %copy-done.2, f32[128]{0:T(128)S(1)} %fusion.2), kind=kOutput, calls=%fused_computation.19 | convolution fusion | flops 608468992 | bytes 13632512 | tf_op jit(solution)/shard_map/dot_general | solution.py:121
  333.9 24.6 %all_to_all.11 = bf16[16,8,2048]{2,1,0:T(8,128)(2,1)S(1)} all-to-all(bf16[16,8,2048]{2,1,0:T(8,128)(2,1)S(1)} %fusion.15), channel_id=1, replica_groups=mesh['grp'=2,'sp'=16,'tp_0'=8,'tp_1'=2] {'tp_0','tp_1'}, dimensions={0} | all-to-all | bytes 1048576 | tf_op jit(solution)/shard_map/all_to_all | solution.py:52
  358.4 0.1 convert_reduce_fusion
  358.5 0.1 multiply_reduce_fusion
  358.6 0.7 add_convert_fusion
  (29 shorter events, 0.5 us)
Async XLA Ops:
  6.5 94.8 %copy-start = (bf16[2,2048,128]{2,1,0:T(8,128)(2,1)S(1)}, bf16[2,2048,128]{2,1,0:T(8,128)(2,1)}, u32[]{:S(2)}) copy-start(bf16[2,2048,128]{2,1,0:T(8,128)(2,1)} %param.10) | copy-start | bytes 3145732
  6.5 86.1 %all-gather.8.cloned.1.call-start = ((), (), s32[]{:S(2)}) async-start(), calls=%async_computation.2 | async-start | bytes 4456448 | tf_op jit(solution)/shard_map/all_gather | solution.py:73
  7.3 97.8 %copy-start.1 = (bf16[2,2048,128]{2,1,0:T(8,128)(2,1)S(1)}, bf16[2,2048,128]{2,1,0:T(8,128)(2,1)}, u32[]{:S(2)}) copy-start(bf16[2,2048,128]{2,1,0:T(8,128)(2,1)} %param.11) | copy-start | bytes 3145732
  7.3 201.0 %all-gather.10.cloned.1.call-start = ((), (), s32[]{:S(2)}) async-start(), calls=%async_computation.3 | async-start | bytes 8912896 | tf_op jit(solution)/shard_map/all_gather | solution.py:37
  100.3 9.6 %copy-start.4 = (bf16[8,2048]{1,0:T(8,128)(2,1)S(1)}, bf16[8,2048]{1,0:T(8,128)(2,1)}, u32[]{:S(2)}) copy-start(bf16[8,2048]{1,0:T(8,128)(2,1)} %param.7) | copy-start | bytes 98308
  100.3 9.7 %copy-start.5 = (f32[2,2,2048]{2,1,0:T(2,128)S(1)}, f32[2,2,2048]{2,1,0:T(2,128)}, u32[]{:S(2)}) copy-start(f32[2,2,2048]{2,1,0:T(2,128)} %param.13) | copy-start | bytes 98308
  101.2 107.1 %copy-start.3 = (bf16[2,2048,128]{2,1,0:T(8,128)(2,1)S(1)}, bf16[2,2048,128]{2,1,0:T(8,128)(2,1)}, u32[]{:S(2)}) copy-start(bf16[2,2048,128]{2,1,0:T(8,128)(2,1)} %param.9) | copy-start | bytes 3145732
  101.3 214.7 %all-gather.12.cloned.1.call-start = ((), (), s32[]{:S(2)}) async-start(), calls=%async_computation.4 | async-start | bytes 8912896 | tf_op jit(solution)/shard_map/all_gather | solution.py:37
  208.4 11.7 %copy-start.2 = (bf16[2,128,2048]{2,1,0:T(8,128)(2,1)S(1)}, bf16[2,128,2048]{2,1,0:T(8,128)(2,1)}, u32[]{:S(2)}) copy-start(bf16[2,128,2048]{2,1,0:T(8,128)(2,1)} %param.12) | copy-start | bytes 3145732
Sparse Core Ops, SparseCore 0:
  9.5 83.0 all-gather.7
  101.4 106.9 all-gather.9
  210.5 105.4 all-gather.11
where the time goes:
time: 366 us
  waiting for transfers between devices  196 us (54%)
  blocking collectives  102 us (28%)
  matrix products  41.7 us (11%)
  between operations  13.3 us (4%)
  other arithmetic  12.8 us (3%)
    all_gather x2, waiting for transfers between devices, sent_together(): lax.all_gather(both, axis, axis=dim, tiled=True)  110 us
    all_gather x1, waiting for transfers between devices, body(): project_shard_part = lax.all_gather(source, TP, axis=0, tiled=True)  85.2 us
    all_gather x4, blocking collectives, stacked_from(): parts = lax.all_gather(parts, axes[k])  52.6 us
    all_to_all x2, blocking collectives, sum_at_owner(): parts = lax.all_to_all(split_up(x, dim, peers), axis, 0, 0, tiled=True)  49.1 us
    dot_general x2, matrix products, body(): jnp.einsum('qhd,khd->hqk', query_heads, key_heads, preferred_element_type...  13.9 us
    dot_general x2, matrix products, body(): jnp.dot(attended, out_weight, preferred_element_type=jnp.float32)  12.7 us
    reduce_sum x2, other arithmetic, body(): row_total = jnp.sum(weights, axis=2)  9.35 us
    dot_general x2, matrix products, body(): jnp.dot(project_shard_part, w_key[level], preferred_element_type=jnp.floa...  7.6 us
  transfers between devices with their start and end apart: 3, of which 3 were waited for; matrix products, arithmetic and copies ran while one was open for 7% of the time, Pallas kernels for 0%

commit v1 on v0

v1 whole, which is shorter than its diff:
```python
import functools

import jax
import jax.numpy as jnp
from jax import lax
from jax.experimental import pallas as pl
from jax.experimental.pallas import tpu as pltpu
from jax.sharding import Mesh
from jax.sharding import PartitionSpec as P

HEAD = 128
EPS = 1e-06
LOG2E = 1.4426950408889634
TP = ("x", "c")
ROWS = ("grp", "sp", "x", "c")
STATS = 8


def split3(v):
    hi = v.astype(jnp.bfloat16).astype(jnp.float32)
    mid = (v - hi).astype(jnp.bfloat16).astype(jnp.float32)
    return hi, mid, v - hi - mid


def attend_kernel(q_ref, k_ref, v_ref, o_ref):
    rows = q_ref.shape[1]
    scores = lax.dot_general(
        q_ref[0], k_ref[...], (((1,), (1,)), ((), ())), preferred_element_type=jnp.float32
    )
    scale = HEAD**-0.5 * LOG2E
    peak = jnp.max(scores, axis=1, keepdims=True)
    weights = jnp.exp2((scores - peak) * scale)
    total = jnp.sum(weights, axis=1, keepdims=True)
    summed = jnp.dot(weights.astype(jnp.bfloat16), v_ref[...], preferred_element_type=jnp.float32)
    o_ref[0, :rows, :] = (summed / total).astype(jnp.bfloat16)
    lane = lax.broadcasted_iota(jnp.int32, (rows, HEAD), 1)
    both = jnp.where(lane < STATS // 2, peak * scale, total)
    flat = jnp.transpose(both)[:STATS]
    hi, mid, low = split3(flat)
    row = lax.broadcasted_iota(jnp.int32, (STATS, rows), 0) % (STATS // 2)
    stats = jnp.where(row == 0, hi, jnp.where(row == 1, mid, low))
    o_ref[0, rows:, :] = stats.astype(jnp.bfloat16)


def attend(queries, projected, level, parts):
    blocks, rows, _ = queries.shape
    sources = projected.shape[0]
    return pl.pallas_call(
        attend_kernel,
        grid=(blocks,),
        in_specs=[
            pl.BlockSpec((1, rows, HEAD), lambda i: (i, 0, 0)),
            pl.BlockSpec((sources, HEAD), lambda i: (0, 2 * level)),
            pl.BlockSpec((sources, HEAD), lambda i: (0, 2 * level + 1)),
        ],
        out_specs=pl.BlockSpec((1, rows + STATS, HEAD), lambda i: (i, 0, 0)),
        out_shape=jax.ShapeDtypeStruct((blocks, rows + STATS, HEAD), jnp.bfloat16),
        cost_estimate=pl.CostEstimate(
            flops=4 * blocks * rows * sources * HEAD,
            bytes_accessed=4 * blocks * rows * HEAD + 4 * sources * HEAD,
            transcendentals=blocks * rows * sources,
        ),
        name="attend",
    )(queries, projected, projected)


def join_kernel(g_ref, o_ref):
    parts, rows = g_ref.shape[0], g_ref.shape[1] - STATS
    half = STATS // 2
    stats = g_ref[:, rows:, :].astype(jnp.float32)
    peaks = stats[:, 0] + stats[:, 1] + stats[:, 2]
    totals = stats[:, half] + stats[:, half + 1] + stats[:, half + 2]
    share = jnp.exp2(peaks - jnp.max(peaks, axis=0, keepdims=True)) * totals
    share = share / jnp.sum(share, axis=0, keepdims=True)
    columns = jnp.transpose(jnp.concatenate([share] * (rows // parts), axis=0))
    joined = jnp.zeros((rows, HEAD), jnp.float32)
    for part in range(parts):
        joined += columns[:, part : part + 1] * g_ref[part, :rows, :].astype(jnp.float32)
    o_ref[...] = joined.astype(jnp.bfloat16)


def join(gathered):
    parts, rows, _ = gathered.shape
    rows -= STATS
    return pl.pallas_call(
        join_kernel,
        out_shape=jax.ShapeDtypeStruct((rows, HEAD), jnp.bfloat16),
        cost_estimate=pl.CostEstimate(
            flops=2 * parts * rows * HEAD, bytes_accessed=2 * parts * rows * HEAD, transcendentals=0
        ),
        name="join",
    )(gathered)


def to_all(block, axis):
    copies = jnp.broadcast_to(block[None], (lax.axis_size(axis), *block.shape))
    return lax.all_to_all(copies, axis, 0, 0, tiled=True)


def normalize(row_block, gain_row):
    return (
        row_block
        * lax.rsqrt(jnp.mean(row_block * row_block, axis=-1, keepdims=True) + EPS)
        * gain_row
    )


def body(target, source, w_query, w_key, w_value, w_out, gains):
    depth, width, _ = w_query.shape
    own = target.shape[0]
    chips, cores = lax.axis_size("x"), lax.axis_size("c")
    block = own * chips * cores
    side = width // cores
    core = lax.axis_index("c")

    rows_here = lax.all_gather(source, TP, axis=0, tiled=True)
    w_sources = jnp.concatenate(
        [w for level in range(depth) for w in (w_key[level], w_value[level])], axis=1
    )
    projected_source = jnp.dot(rows_here, w_sources, preferred_element_type=jnp.float32).astype(
        jnp.bfloat16
    )
    w_mix = w_out.reshape(depth, HEAD, cores, side).transpose(2, 0, 1, 3)
    w_mix = lax.all_to_all(w_mix, "c", 0, 0, tiled=True)

    stream = target.astype(jnp.float32)
    for level in range(depth):
        normed = normalize(stream, gains[level, 0]).astype(jnp.bfloat16)
        normed = lax.all_gather(to_all(normed, "x"), "c").reshape(block, width)
        queries = jnp.dot(normed, w_query[level], preferred_element_type=jnp.float32)
        queries = to_all(queries.astype(jnp.bfloat16), "sp")
        partial = attend(queries, projected_source, level, lax.axis_size("sp"))
        attended = join(lax.all_to_all(partial, "sp", 0, 0, tiled=True))
        pair = lax.all_gather(attended, "c")
        mixed = sum(
            jnp.dot(pair[k], w_mix[k, level], preferred_element_type=jnp.float32)
            for k in range(cores)
        ).astype(jnp.bfloat16)
        mixed = mixed.reshape(cores, chips, own, side).transpose(1, 0, 2, 3)
        mixed = lax.all_to_all(mixed, "x", 0, 0, tiled=True)
        mixed = jnp.sum(mixed.astype(jnp.float32), axis=0)
        mixed = lax.all_gather(mixed, "c")
        mixed = lax.dynamic_index_in_dim(mixed, core, 1, keepdims=False)
        projected = mixed.transpose(1, 0, 2).reshape(own, width)
        stream = stream + normalize(projected, gains[level, 1])
    return stream.astype(jnp.bfloat16)


def solution(mesh):
    split = Mesh(
        mesh.devices.reshape(mesh.shape["grp"], mesh.shape["sp"], -1, 2), ROWS
    )
    placed = (
        P(ROWS, None),
        P(ROWS, None),
        P(None, None, TP),
        P(None, None, TP),
        P(None, None, TP),
        P(None, TP, None),
        P(),
    )
    return jax.shard_map(
        body, mesh=split, in_specs=placed, out_specs=P(ROWS, None), check_vma=False
    )
```

time: 366 us -> 323 us (0.88)
  waiting for transfers between devices: 196 us -> 50.3 us
  blocking collectives: 102 us -> 174 us
  starting transfers between devices: 0.13 us -> 36.6 us
  matrix products: 41.7 us -> 8.46 us
  Pallas kernels: 0 us -> 28.2 us
  other arithmetic: 12.8 us -> 3.1 us
  local copies, waits for them, and re-layouts: 0.2 us -> 6.34 us
    all_gather x3 -> x1, waiting for transfers between devices: 195 us -> 13.4 us  [body(): rows_here = lax.all_gather(source, TP, axis=0, tiled=True)]
    all_to_all x2 -> x5, blocking collectives: 49.1 us -> 121 us  [the longest x3 61.1 us: to_all(): return lax.all_to_all(copies, axis, 0, 0, tiled=True)]
    all_to_all x0 -> x4, starting transfers between devices: none -> 36.6 us  [the longest x1 13 us: body(): attended = join(lax.all_to_all(partial, 'sp', 0, 0, tiled=True))]
    all_to_all x0 -> x4, waiting for transfers between devices: none -> 36.2 us  [the longest x1 22.1 us: body(): attended = join(lax.all_to_all(partial, 'sp', 0, 0, tiled=True))]
    dot_general x8 -> x7, matrix products: 41.7 us -> 8.46 us  [the longest x1 5.93 us: body(): jnp.dot(rows_here, w_sources, preferred_element_type=jnp.float32)]
    pallas_call x0 -> x4, Pallas kernels: none -> 28.2 us  [the longest x2 23.7 us: attend(): pl.pallas_call(attend_kernel, grid=(blocks,), in_specs=[pl.BlockSpec((1,...]
    reduce_sum x4 -> x2, other arithmetic: 9.5 us -> 0.08 us  [body(): mixed = jnp.sum(mixed.astype(jnp.float32), axis=0)]
    all_gather x4 -> x6, blocking collectives: 52.6 us -> 52.4 us  [the longest x2 41.5 us: body(): normed = lax.all_gather(to_all(normed, 'x'), 'c').reshape(block, width)]
  transfers between devices with their start and end apart: 3 -> 5, of which waited for: 3 -> 4; matrix products, arithmetic and copies ran while one was open for 7% -> 4% of each run, Pallas kernels for 0% -> 1%
where the time goes in v1:
time: 323 us; the launch traced here: 320 us
  blocking collectives  174 us (54%)
  waiting for transfers between devices  50.3 us (16%)
  starting transfers between devices  36.6 us (11%)
  Pallas kernels  28.2 us (9%)
  between operations  13.6 us (4%)
  matrix products  8.46 us (3%)
  local copies, waits for them, and re-layouts  6.34 us (2%)
    all_to_all x3, blocking collectives, to_all(): return lax.all_to_all(copies, axis, 0, 0, tiled=True)  61.1 us
    all_to_all x1, blocking collectives, body(): attended = join(lax.all_to_all(partial, 'sp', 0, 0, tiled=True))  45.3 us
    all_gather x2, blocking collectives, body(): normed = lax.all_gather(to_all(normed, 'x'), 'c').reshape(block, width)  41.5 us
    pallas_call x2, Pallas kernels, attend(): pl.pallas_call(attend_kernel, grid=(blocks,), in_specs=[pl.BlockSpec((1,...  23.7 us
    all_to_all x1, waiting for transfers between devices, body(): attended = join(lax.all_to_all(partial, 'sp', 0, 0, tiled=True))  22.1 us
    all_to_all x1, blocking collectives, body(): mixed = lax.all_to_all(mixed, 'x', 0, 0, tiled=True)  14.8 us
    all_gather x1, waiting for transfers between devices, body(): rows_here = lax.all_gather(source, TP, axis=0, tiled=True)  13.4 us
    all_to_all x1, starting transfers between devices, body(): attended = join(lax.all_to_all(partial, 'sp', 0, 0, tiled=True))  13 us
  transfers between devices with their start and end apart: 5, of which 4 were waited for; matrix products, arithmetic and copies ran while one was open for 4% of the time, Pallas kernels for 1%

profile of v1, /device:TPU:65, one launch (start us, length us, event | category | flops | bytes accessed | tf_op | source)
XLA Modules:
  0.0 320.2 jit_solution(2843238559881578200)
XLA Ops:
  7.3 0.9 fusion.24
  8.2 0.8 fusion.34
  9.0 0.8 fusion.26
  9.9 17.0 %all_to_all.45 = bf16[8,8,2048]{2,1,0:T(8,128)(2,1)S(1)} all-to-all(bf16[8,8,2048]{2,1,0:T(8,128)(2,1)S(1)} %broadcast_in_dim.8), channel_id=1, replica_groups=mesh['grp'=2,'sp'=16,'x'=8,'c'=2] {'x'}, dimensions={0} | all-to-all | bytes 524288 | tf_op jit(solution)/shard_map/all_to_all | solution.py:97
  26.9 39.2 %all-gather = bf16[16,8,2048]{2,1,0:T(8,128)(2,1)S(1)} all-gather(bf16[8,8,2048]{2,1,0:T(8,128)(2,1)S(1)} %all_to_all.45), channel_id=2, replica_groups=mesh['grp'=2,'sp'=16,'x'=8,'c'=2] {'c'}, dimensions={0}, use_global_device_ids=true | all-gather | bytes 786432 | tf_op jit(solution)/shard_map/all_gather | solution.py:129
  66.1 1.3 convolution_convert_fusion.1
  67.4 0.9 broadcast_in_dim.9
  68.3 9.7 %all-to-all-start.1 = ((bf16[16,128,128]{2,1,0:T(8,128)(2,1)}), bf16[16,128,128]{2,1,0:T(8,128)(2,1)S(1)}, u32[]{:S(2)}, u32[]{:S(2)}) async-start(bf16[16,128,128]{2,1,0:T(8,128)(2,1)} %broadcast_in_dim.9), calls=%async_computation.1 | async-start | bytes 1048576 | tf_op jit(solution)/shard_map/all_to_all | solution.py:97
  78.0 1.2 slice_bitcast_fusion.2
  79.2 13.4 %all-gather.8.cloned.1.call-done = bf16[1024,2048]{1,0:T(8,128)(2,1)} async-done(((bf16[64,2048]{1,0:T(8,128)(2,1)}), bf16[1024,2048]{1,0:T(8,128)(2,1)}) %all-gather.8.cloned.1.call-update) | async-done | bytes 4194320 | tf_op jit(solution)/shard_map/all_gather | solution.py:116
  92.6 5.9 %fusion.11.k_ref.v_ref = bf16[1024,512]{1,0:T(8,128)(2,1)} fusion(bf16[1024,2048]{1,0:T(8,128)(2,1)} %all-gather.8.cloned.1.call-done, bf16[2048,128]{1,0:T(8,128)(2,1)} %get-tuple-element.12, bf16[2048,128]{1,0:T(8,128)(2,1)} %get-tuple-element.17, bf16[2048,128]{1,0:T(8,128)(2,1)S(1)} %get-tuple-element.11, bf16[2048,128]{1,0:T(8,128)(2,1)} %get-tuple-element.18), kind=kOutput, calls=%fused_computation.9 | convolution fusion | flops 2156396544 | bytes 7340032 | tf_op jit(solution)/shard_map/dot_general | solution.py:120
  98.5 2.0 all-to-all-done.1.q_ref
  100.5 0.8 copy-done.5
  101.3 11.9 %attend.2 = bf16[16,136,128]{2,1,0:T(8,128)(2,1)} custom-call(bf16[16,128,128]{2,1,0:T(8,128)(2,1)} %copy-done.5, bf16[1024,512]{1,0:T(8,128)(2,1)} %fusion.11.k_ref.v_ref, bf16[1024,512]{1,0:T(8,128)(2,1)} %fusion.11.k_ref.v_ref), custom_call_target="tpu_custom_call" | custom-call | flops 1073741824 | bytes 1572864 | tf_op jit(solution)/shard_map/attend/pallas_call | solution.py:48
  113.2 13.0 %all-to-all-start.2 = ((bf16[16,136,128]{2,1,0:T(8,128)(2,1)}), bf16[16,136,128]{2,1,0:T(8,128)(2,1)S(1)}, u32[]{:S(2)}, u32[]{:S(2)}) async-start(bf16[16,136,128]{2,1,0:T(8,128)(2,1)} %attend.2), calls=%async_computation.2 | async-start | bytes 1114112 | tf_op jit(solution)/shard_map/all_to_all | solution.py:133
  126.9 1.0 copy.18
  128.0 22.1 %all-to-all-done.2.g_ref = bf16[16,136,128]{2,1,0:T(8,128)(2,1)S(1)} async-done(((bf16[16,136,128]{2,1,0:T(8,128)(2,1)}), bf16[16,136,128]{2,1,0:T(8,128)(2,1)S(1)}, u32[]{:S(2)}, u32[]{:S(2)}) %all-to-all-start.2) | async-done | bytes 557088 | tf_op jit(solution)/shard_map/all_to_all | solution.py:133
  150.1 10.3 %all-to-all-start.3 = ((bf16[2,2,128,1024]{2,3,1,0:T(8,128)(2,1)}), bf16[2,2,128,1024]{2,3,1,0:T(8,128)(2,1)S(1)}, u32[]{:S(2)}, u32[]{:S(2)}) async-start(bf16[2,2,128,1024]{2,3,1,0:T(8,128)(2,1)} %copy.18), calls=%async_computation.3 | async-start | bytes 2097152 | tf_op jit(solution)/shard_map/all_to_all | solution.py:124
  160.4 2.2 join.2
  162.6 2.1 all-gather.1
  165.9 3.6 %all-to-all-start.4 = ((bf16[8,2,8,1024]{3,2,1,0:T(8,128)(2,1)}), bf16[8,2,8,1024]{3,2,1,0:T(8,128)(2,1)S(1)}, u32[]{:S(2)}, u32[]{:S(2)}) async-start(bf16[8,2,8,1024]{3,2,1,0:T(8,128)(2,1)} %bitcast.71), calls=%async_computation.4 | async-start | bytes 524288 | tf_op jit(solution)/shard_map/all_to_all | solution.py:140
  169.5 12.1 %all-to-all-done.4 = bf16[8,2,8,1024]{3,2,1,0:T(8,128)(2,1)S(1)} async-done(((bf16[8,2,8,1024]{3,2,1,0:T(8,128)(2,1)}), bf16[8,2,8,1024]{3,2,1,0:T(8,128)(2,1)S(1)}, u32[]{:S(2)}, u32[]{:S(2)}) %all-to-all-start.4) | async-done | bytes 262176 | tf_op jit(solution)/shard_map/all_to_all | solution.py:140
  181.6 2.1 all-gather.2
  184.2 14.8 %all_to_all.46 = bf16[8,8,2048]{2,1,0:T(8,128)(2,1)S(1)} all-to-all(bf16[8,8,2048]{2,1,0:T(8,128)(2,1)S(1)} %broadcast_in_dim.10), channel_id=1, replica_groups=mesh['grp'=2,'sp'=16,'x'=8,'c'=2] {'x'}, dimensions={0} | all-to-all | bytes 524288 | tf_op jit(solution)/shard_map/all_to_all | solution.py:97
  199.0 2.3 all-gather.3
  201.7 29.4 %all_to_all.47.q_ref = bf16[16,128,128]{2,1,0:T(8,128)(2,1)} all-to-all(bf16[16,128,128]{2,1,0:T(8,128)(2,1)S(1)} %broadcast_in_dim.11), channel_id=1, replica_groups=mesh['grp'=2,'sp'=16,'x'=8,'c'=2] {'sp'}, dimensions={0} | all-to-all | bytes 1048576 | tf_op jit(solution)/shard_map/all_to_all | solution.py:97
  231.1 11.9 %attend.3 = bf16[16,136,128]{2,1,0:T(8,128)(2,1)} custom-call(bf16[16,128,128]{2,1,0:T(8,128)(2,1)} %all_to_all.47.q_ref, bf16[1024,512]{1,0:T(8,128)(2,1)} %fusion.11.k_ref.v_ref, bf16[1024,512]{1,0:T(8,128)(2,1)} %fusion.11.k_ref.v_ref), custom_call_target="tpu_custom_call" | custom-call | flops 1073741824 | bytes 1572864 | tf_op jit(solution)/shard_map/attend/pallas_call | solution.py:48
  243.0 45.3 %all_to_all.48.g_ref = bf16[16,136,128]{2,1,0:T(8,128)(2,1)} all-to-all(bf16[16,136,128]{2,1,0:T(8,128)(2,1)} %attend.3), channel_id=1, replica_groups=mesh['grp'=2,'sp'=16,'x'=8,'c'=2] {'sp'}, dimensions={0} | all-to-all | bytes 1114112 | tf_op jit(solution)/shard_map/all_to_all | solution.py:133
  288.3 2.2 join.3
  290.5 4.6 %all-gather.4 = bf16[256,128]{1,0:T(8,128)(2,1)S(1)} all-gather(bf16[128,128]{1,0:T(8,128)(2,1)} %join.3), channel_id=6, replica_groups=mesh['grp'=2,'sp'=16,'x'=8,'c'=2] {'c'}, dimensions={0}, use_global_device_ids=true | all-gather | bytes 98304 | tf_op jit(solution)/shard_map/all_gather | solution.py:134
  295.6 14.8 %all_to_all.49 = bf16[8,2,8,1024]{3,2,1,0:T(8,128)(2,1)S(1)} all-to-all(bf16[8,2,8,1024]{3,2,1,0:T(8,128)(2,1)S(1)} %bitcast.73), channel_id=1, replica_groups=mesh['grp'=2,'sp'=16,'x'=8,'c'=2] {'x'}, dimensions={0} | all-to-all | bytes 524288 | tf_op jit(solution)/shard_map/all_to_all | solution.py:140
  310.4 2.1 all-gather.5
  (38 shorter events, 4.9 us)
Async XLA Ops:
  6.5 71.5 %copy-start.3 = (bf16[2,2048,128]{2,1,0:T(8,128)(2,1)S(1)}, bf16[2,2048,128]{2,1,0:T(8,128)(2,1)}, u32[]{:S(2)}) copy-start(bf16[2,2048,128]{2,1,0:T(8,128)(2,1)} %param.10) | copy-start | bytes 3145732
  6.5 71.5 %copy-start.2 = (bf16[2,2048,128]{2,1,0:T(8,128)(2,1)S(1)}, bf16[2,2048,128]{2,1,0:T(8,128)(2,1)}, u32[]{:S(2)}) copy-start(bf16[2,2048,128]{2,1,0:T(8,128)(2,1)} %param.11) | copy-start | bytes 3145732
  6.6 86.1 %all-gather.8.cloned.1.call-start = ((), (), s32[]{:S(2)}) async-start(), calls=%async_computation.9 | async-start | bytes 4456448 | tf_op jit(solution)/shard_map/all_gather | solution.py:116
  68.3 32.2 %all-to-all-start.1 = ((bf16[16,128,128]{2,1,0:T(8,128)(2,1)}), bf16[16,128,128]{2,1,0:T(8,128)(2,1)S(1)}, u32[]{:S(2)}, u32[]{:S(2)}) async-start(bf16[16,128,128]{2,1,0:T(8,128)(2,1)} %broadcast_in_dim.9), calls=%async_computation.1 | async-start | bytes 1048576 | tf_op jit(solution)/shard_map/all_to_all | solution.py:97
  98.5 27.7 %copy-start.1 = (bf16[2,128,2048]{2,1,0:T(8,128)(2,1)S(1)}, bf16[2,128,2048]{2,1,0:T(8,128)(2,1)}, u32[]{:S(2)}) copy-start(bf16[2,128,2048]{2,1,0:T(8,128)(2,1)} %param.12) | copy-start | bytes 3145732
  100.5 0.8 copy-start.5
  113.2 36.9 %all-to-all-start.2 = ((bf16[16,136,128]{2,1,0:T(8,128)(2,1)}), bf16[16,136,128]{2,1,0:T(8,128)(2,1)S(1)}, u32[]{:S(2)}, u32[]{:S(2)}) async-start(bf16[16,136,128]{2,1,0:T(8,128)(2,1)} %attend.2), calls=%async_computation.2 | async-start | bytes 1114112 | tf_op jit(solution)/shard_map/all_to_all | solution.py:133
  126.9 56.9 %copy-start.4 = (bf16[8,2048]{1,0:T(8,128)(2,1)S(1)}, bf16[8,2048]{1,0:T(8,128)(2,1)}, u32[]{:S(2)}) copy-start(bf16[8,2048]{1,0:T(8,128)(2,1)} %param.7) | copy-start | bytes 98308
  128.0 73.3 %copy-start.6 = (bf16[2,2048,128]{2,1,0:T(8,128)(2,1)S(1)}, bf16[2,2048,128]{2,1,0:T(8,128)(2,1)}, u32[]{:S(2)}) copy-start(bf16[2,2048,128]{2,1,0:T(8,128)(2,1)} %param.9) | copy-start | bytes 3145732
  150.1 10.3 %copy-start = (bf16[16,136,128]{2,1,0:T(8,128)(2,1)}, bf16[16,136,128]{2,1,0:T(8,128)(2,1)S(1)}, u32[]{:S(2)}) copy-start(bf16[16,136,128]{2,1,0:T(8,128)(2,1)S(1)} %all-to-all-done.2.g_ref) | copy-start | bytes 1671172
  150.1 14.6 %all-to-all-start.3 = ((bf16[2,2,128,1024]{2,3,1,0:T(8,128)(2,1)}), bf16[2,2,128,1024]{2,3,1,0:T(8,128)(2,1)S(1)}, u32[]{:S(2)}, u32[]{:S(2)}) async-start(bf16[2,2,128,1024]{2,3,1,0:T(8,128)(2,1)} %copy.18), calls=%async_computation.3 | async-start | bytes 2097152 | tf_op jit(solution)/shard_map/all_to_all | solution.py:124
  165.9 15.7 %all-to-all-start.4 = ((bf16[8,2,8,1024]{3,2,1,0:T(8,128)(2,1)}), bf16[8,2,8,1024]{3,2,1,0:T(8,128)(2,1)S(1)}, u32[]{:S(2)}, u32[]{:S(2)}) async-start(bf16[8,2,8,1024]{3,2,1,0:T(8,128)(2,1)} %bitcast.71), calls=%async_computation.4 | async-start | bytes 524288 | tf_op jit(solution)/shard_map/all_to_all | solution.py:140
Sparse Core Ops, SparseCore 0:
  9.5 83.0 all-gather.7

commit v2 on v1

v2 whole, which is shorter than its diff:
```python
import functools

import jax
import jax.numpy as jnp
from jax import lax
from jax.experimental import pallas as pl
from jax.experimental.pallas import tpu as pltpu
from jax.sharding import Mesh
from jax.sharding import PartitionSpec as P

HEAD = 128
EPS = 1e-06
LOG2E = 1.4426950408889634
TP = ("x", "c")
SP = ("far", "near")
ROWS = ("grp", "far", "near", "x", "c")
STATS = 8
BLOCK = 128
NEAR = 4


def split3(v):
    hi = v.astype(jnp.bfloat16).astype(jnp.float32)
    mid = (v - hi).astype(jnp.bfloat16).astype(jnp.float32)
    return hi, mid, v - hi - mid


def attend_kernel(rows, chunk, q_ref, k_ref, v_ref, o_ref, values_ref):
    sources = k_ref.shape[0]
    scale = HEAD**-0.5 * LOG2E
    half = STATS // 2
    values_ref[...] = jnp.transpose(v_ref[...].astype(jnp.float32)).astype(jnp.bfloat16)

    def step(index, carry):
        queries = q_ref[pl.ds(pl.multiple_of(index * rows, rows), rows), :]
        peak = total = out = None
        for at in range(0, sources, chunk):
            scores = lax.dot_general(
                k_ref[at : at + chunk, :],
                queries,
                (((1,), (1,)), ((), ())),
                preferred_element_type=jnp.float32,
            )
            top = jnp.max(scores, axis=0, keepdims=True)
            new = top if peak is None else jnp.maximum(peak, top)
            weights = jnp.exp2((scores - new) * scale)
            here = jnp.sum(weights, axis=0, keepdims=True)
            part = jnp.dot(
                values_ref[:, at : at + chunk],
                weights.astype(jnp.bfloat16),
                preferred_element_type=jnp.float32,
            )
            if peak is None:
                total, out = here, part
            else:
                fade = jnp.exp2((peak - new) * scale)
                total, out = total * fade + here, out * fade + part
            peak = new
        out = (out / total).astype(jnp.bfloat16)
        row = lax.broadcasted_iota(jnp.int32, (STATS, rows), 0)
        hi, mid, low = split3(jnp.where(row < half, peak * scale, total))
        stats = jnp.where(row % half == 0, hi, jnp.where(row % half == 1, mid, low))
        stats = stats.astype(jnp.bfloat16)
        first = index * (rows // BLOCK)
        for k in range(rows // BLOCK):
            lanes = slice(k * BLOCK, (k + 1) * BLOCK)
            o_ref[first + k, :HEAD, :] = out[:, lanes]
            o_ref[first + k, HEAD:, :] = stats[:, lanes]
        return carry

    lax.fori_loop(0, q_ref.shape[0] // rows, step, 0)


def attend(queries, projected):
    rows, sources = queries.shape[0], projected.shape[0]
    blocks = rows // BLOCK
    out = (blocks, HEAD + STATS, BLOCK)
    return pl.pallas_call(
        functools.partial(attend_kernel, min(rows, 512), min(sources, 1024)),
        grid=(1,),
        in_specs=[
            pl.BlockSpec((rows, HEAD), lambda i: (0, 0)),
            pl.BlockSpec((sources, HEAD), lambda i: (0, 0)),
            pl.BlockSpec((sources, HEAD), lambda i: (0, 1)),
        ],
        out_specs=pl.BlockSpec(out, lambda i: (0, 0, 0)),
        out_shape=jax.ShapeDtypeStruct(out, jnp.bfloat16),
        scratch_shapes=[pltpu.VMEM((HEAD, sources), jnp.bfloat16)],
        compiler_params=pltpu.CompilerParams(vmem_limit_bytes=32 * 2**20),
        cost_estimate=pl.CostEstimate(
            flops=4 * rows * sources * HEAD,
            bytes_accessed=4 * rows * HEAD + 4 * sources * HEAD,
            transcendentals=rows * sources,
        ),
        name="attend",
    )(queries, projected, projected)


def join_kernel(g_ref, o_ref):
    half = STATS // 2
    stats = g_ref[:, HEAD:, :].astype(jnp.float32)
    peaks = stats[:, 0] + stats[:, 1] + stats[:, 2]
    totals = stats[:, half] + stats[:, half + 1] + stats[:, half + 2]
    share = jnp.exp2(peaks - jnp.max(peaks, axis=0, keepdims=True)) * totals
    share = share / jnp.sum(share, axis=0, keepdims=True)
    joined = jnp.zeros((HEAD, BLOCK), jnp.float32)
    for part in range(g_ref.shape[0]):
        joined += share[part : part + 1] * g_ref[part, :HEAD, :].astype(jnp.float32)
    o_ref[...] = joined.astype(jnp.bfloat16)


def join(gathered):
    return pl.pallas_call(
        join_kernel,
        out_shape=jax.ShapeDtypeStruct((HEAD, BLOCK), jnp.bfloat16),
        cost_estimate=pl.CostEstimate(
            flops=2 * gathered.size, bytes_accessed=2 * gathered.size, transcendentals=0
        ),
        name="join",
    )(gathered)


def to_all(block, axis):
    copies = jnp.broadcast_to(block[None], (lax.axis_size(axis), *block.shape))
    return lax.all_to_all(copies, axis, 0, 0, tiled=True)


def normalize(row_block, gain_row):
    return (
        row_block
        * lax.rsqrt(jnp.mean(row_block * row_block, axis=-1, keepdims=True) + EPS)
        * gain_row
    )


def dot(a, b):
    return jnp.dot(a, b, preferred_element_type=jnp.float32)


def body(target, source, w_query, w_key, w_value, w_out, gains):
    depth, width, _ = w_query.shape
    own = target.shape[0]
    chips, cores = lax.axis_size("x"), lax.axis_size("c")
    block = own * chips * cores
    side = width // cores
    core = lax.axis_index("c")

    rows_here = lax.all_gather(source, TP, axis=0, tiled=True)
    projected_source = []
    for level in range(depth):
        both = jnp.concatenate([w_key[level], w_value[level]], axis=1)
        both = dot(rows_here, both).astype(jnp.bfloat16)
        if level > 0:
            both = lax.all_gather(both, "near", axis=0, tiled=True)
        projected_source.append(both)

    mine = lax.dynamic_slice_in_dim(w_out, core * side, side, 2)
    other = lax.dynamic_slice_in_dim(w_out, (1 - core) * side, side, 2)
    other = lax.ppermute(other, "c", [(0, 1), (1, 0)])
    w_mix = jnp.concatenate(
        [jnp.where(core == 0, mine, other), jnp.where(core == 0, other, mine)], axis=1
    )

    stream = target.astype(jnp.float32)
    for level in range(depth):
        normed = normalize(stream, gains[level, 0]).astype(jnp.bfloat16)
        normed = lax.all_gather(to_all(normed, "x"), "c").reshape(block, width)
        peers = SP if level == 0 else "far"
        queries = to_all(dot(normed, w_query[level]).astype(jnp.bfloat16), peers)
        if level == 0:
            queries, w_mix = lax.optimization_barrier((queries, w_mix))
        partial = attend(queries.reshape(-1, HEAD), projected_source[level])
        attended = join(lax.all_to_all(partial, peers, 0, 0, tiled=True))
        pair = lax.all_gather(attended, "c", axis=0, tiled=True)
        mixed = lax.dot_general(
            pair, w_mix[level], (((0,), (0,)), ((), ())), preferred_element_type=jnp.float32
        ).astype(jnp.bfloat16)
        mixed = mixed.reshape(cores, chips, own, side).transpose(1, 0, 2, 3)
        mixed = lax.all_to_all(mixed, "x", 0, 0, tiled=True)
        mixed = jnp.sum(mixed.astype(jnp.float32), axis=0)
        mixed = lax.all_gather(mixed, "c")
        mixed = lax.dynamic_index_in_dim(mixed, core, 1, keepdims=False)
        projected = mixed.transpose(1, 0, 2).reshape(own, width)
        stream = stream + normalize(projected, gains[level, 1])
    return stream.astype(jnp.bfloat16)


def solution(mesh):
    split = Mesh(
        mesh.devices.reshape(mesh.shape["grp"], mesh.shape["sp"] // NEAR, NEAR, -1, 2), ROWS
    )
    placed = (
        P(ROWS, None),
        P(ROWS, None),
        P(None, None, TP),
        P(None, None, TP),
        P(None, None, TP),
        P(None, TP, None),
        P(),
    )
    return jax.shard_map(
        body, mesh=split, in_specs=placed, out_specs=P(ROWS, None), check_vma=False
    )
```

time: 323 us -> 272 us (0.84)
  blocking collectives: 174 us -> 123 us
  Pallas kernels: 28.2 us -> 12.4 us
  waiting for transfers between devices: 50.3 us -> 60.4 us
    all_to_all x3 -> x2, blocking collectives: 61.1 us -> 31.9 us  [to_all(): return lax.all_to_all(copies, axis, 0, 0, tiled=True)]
    all_to_all x1, blocking collectives: 45.3 us -> 18 us  [body(): attended = join(lax.all_to_all(partial, peers, 0, 0, tiled=True))]
    all_to_all x1 -> x2, waiting for transfers between devices: 2 us -> 28.1 us  [to_all(): return lax.all_to_all(copies, axis, 0, 0, tiled=True)]
    pallas_call x4, Pallas kernels: 28.2 us -> 12.4 us  [the longest x2 9.01 us: attend(): pl.pallas_call(functools.partial(attend_kernel, min(rows, 512), min(sourc...]
    all_gather x1, waiting for transfers between devices: 13.4 us -> 0.01 us  [body(): rows_here = lax.all_gather(source, TP, axis=0, tiled=True)]
    all_to_all x2 -> x1, starting transfers between devices: 23.3 us -> 13 us  [body(): attended = join(lax.all_to_all(partial, peers, 0, 0, tiled=True))]
    all_to_all x1 -> x2, starting transfers between devices: 9.66 us -> 19.2 us  [to_all(): return lax.all_to_all(copies, axis, 0, 0, tiled=True)]
    all_gather x2, blocking collectives: 6.72 us -> 12.8 us  [body(): pair = lax.all_gather(attended, 'c', axis=0, tiled=True)]
  transfers between devices with their start and end apart: 5 -> 7, of which waited for: 4 -> 4; matrix products, arithmetic and copies ran while one was open for 4% -> 6% of each run, Pallas kernels for 1% -> 1%
where the time goes in v2:
time: 272 us; the launch traced here: 271 us
  blocking collectives  123 us (45%)
  waiting for transfers between devices  60.4 us (22%)
  starting transfers between devices  38.5 us (14%)
  between operations  13.7 us (5%)
  Pallas kernels  12.4 us (5%)
  matrix products  9.82 us (4%)
  local copies, waits for them, and re-layouts  8.23 us (3%)
  other arithmetic  4.57 us (2%)
    all_gather x2, blocking collectives, body(): normed = lax.all_gather(to_all(normed, 'x'), 'c').reshape(block, width)  41.6 us
    all_to_all x2, blocking collectives, to_all(): return lax.all_to_all(copies, axis, 0, 0, tiled=True)  31.9 us
    all_to_all x2, waiting for transfers between devices, to_all(): return lax.all_to_all(copies, axis, 0, 0, tiled=True)  28.1 us
    all_to_all x1, waiting for transfers between devices, body(): attended = join(lax.all_to_all(partial, peers, 0, 0, tiled=True))  19.4 us
    all_to_all x2, starting transfers between devices, to_all(): return lax.all_to_all(copies, axis, 0, 0, tiled=True)  19.2 us
    all_to_all x1, blocking collectives, body(): attended = join(lax.all_to_all(partial, peers, 0, 0, tiled=True))  18 us
    all_to_all x1, blocking collectives, body(): mixed = lax.all_to_all(mixed, 'x', 0, 0, tiled=True)  14.8 us
    all_to_all x1, starting transfers between devices, body(): attended = join(lax.all_to_all(partial, peers, 0, 0, tiled=True))  13 us
  transfers between devices with their start and end apart: 7, of which 4 were waited for; matrix products, arithmetic and copies ran while one was open for 6% of the time, Pallas kernels for 1%

profile of v2, /device:TPU:65, one launch (start us, length us, event | category | flops | bytes accessed | tf_op | source)
XLA Modules:
  0.0 270.9 jit_solution(14901865485241601723)
XLA Ops:
  7.3 0.9 fusion.18
  9.0 0.8 fusion.20
  9.9 17.1 %all_to_all.40 = bf16[8,8,2048]{2,1,0:T(8,128)(2,1)S(1)} all-to-all(bf16[8,8,2048]{2,1,0:T(8,128)(2,1)S(1)} %broadcast_in_dim.8), channel_id=1, replica_groups=mesh['grp'=2,'far'=4,'near'=4,'x'=8,'c'=2] {'x'}, dimensions={0} | all-to-all | bytes 524288 | tf_op jit(solution)/shard_map/all_to_all | solution.py:125
  27.0 39.3 %all-gather = bf16[16,8,2048]{2,1,0:T(8,128)(2,1)S(1)} all-gather(bf16[8,8,2048]{2,1,0:T(8,128)(2,1)S(1)} %all_to_all.40), channel_id=2, replica_groups=mesh['grp'=2,'far'=4,'near'=4,'x'=8,'c'=2] {'c'}, dimensions={0}, use_global_device_ids=true | all-gather | bytes 786432 | tf_op jit(solution)/shard_map/all_gather | solution.py:167
  66.3 1.3 convolution_convert_fusion.5
  67.7 0.9 broadcast_in_dim.9
  68.6 9.7 %all-to-all-start.1 = ((bf16[16,128,128]{2,1,0:T(8,128)(2,1)}), bf16[16,128,128]{2,1,0:T(8,128)(2,1)S(1)}, u32[]{:S(2)}, u32[]{:S(2)}) async-start(bf16[16,128,128]{2,1,0:T(8,128)(2,1)} %broadcast_in_dim.9), calls=%async_computation.1 | async-start | bytes 1048576 | tf_op jit(solution)/shard_map/all_to_all | solution.py:125
  78.4 2.6 collective-permute-start
  81.0 2.6 slice_bitcast_fusion
  83.6 1.4 broadcast_select_fusion.1
  85.1 15.8 %all-to-all-done.1 = bf16[16,128,128]{2,1,0:T(8,128)(2,1)S(1)} async-done(((bf16[16,128,128]{2,1,0:T(8,128)(2,1)}), bf16[16,128,128]{2,1,0:T(8,128)(2,1)S(1)}, u32[]{:S(2)}, u32[]{:S(2)}) %all-to-all-start.1) | async-done | bytes 524320 | tf_op jit(solution)/shard_map/all_to_all | solution.py:125
  100.9 3.4 %fusion.k_ref.v_ref = bf16[1024,256]{1,0:T(8,128)(2,1)S(1)} fusion(bf16[1024,2048]{1,0:T(8,128)(2,1)} %all-gather.7.cloned.1.call-done, bf16[2048,128]{1,0:T(8,128)(2,1)S(1)} %copy-done.7, bf16[2048,128]{1,0:T(8,128)(2,1)S(1)} %copy-done.8), kind=kOutput, calls=%fused_computation.2 | convolution fusion | flops 1076101120 | bytes 5767168 | tf_op jit(solution)/shard_map/dot_general | solution.py:137
  104.4 5.2 %attend.2 = bf16[16,136,128]{2,1,0:T(8,128)(2,1)} custom-call(bf16[2048,128]{1,0:T(8,128)(2,1)S(1)} %bitcast.67, bf16[1024,256]{1,0:T(8,128)(2,1)S(1)} %fusion.k_ref.v_ref, bf16[1024,256]{1,0:T(8,128)(2,1)S(1)} %fusion.k_ref.v_ref), custom_call_target="tpu_custom_call" | custom-call | flops 1073741824 | bytes 1572864 | tf_op jit(solution)/shard_map/attend/pallas_call | solution.py:78
  109.6 13.0 %all-to-all-start.2 = ((bf16[16,136,128]{2,1,0:T(8,128)(2,1)}), bf16[16,136,128]{2,1,0:T(8,128)(2,1)S(1)}, u32[]{:S(2)}, u32[]{:S(2)}) async-start(bf16[16,136,128]{2,1,0:T(8,128)(2,1)} %attend.2), calls=%async_computation.2 | async-start | bytes 1114112 | tf_op jit(solution)/shard_map/all_to_all | solution.py:173
  122.7 4.2 %fusion.1 = bf16[1024,256]{1,0:T(8,128)(2,1)} fusion(bf16[1024,2048]{1,0:T(8,128)(2,1)} %all-gather.7.cloned.1.call-done, bf16[2048,128]{1,0:T(8,128)(2,1)S(1)} %copy-done.5, bf16[2048,128]{1,0:T(8,128)(2,1)S(1)} %copy-done.6), kind=kOutput, calls=%fused_computation.3 | convolution fusion | flops 1076101120 | bytes 5767168 | tf_op jit(solution)/shard_map/dot_general | solution.py:137
  127.0 19.4 %all-to-all-done.2.g_ref = bf16[16,136,128]{2,1,0:T(8,128)(2,1)S(1)} async-done(((bf16[16,136,128]{2,1,0:T(8,128)(2,1)}), bf16[16,136,128]{2,1,0:T(8,128)(2,1)S(1)}, u32[]{:S(2)}, u32[]{:S(2)}) %all-to-all-start.2) | async-done | bytes 557088 | tf_op jit(solution)/shard_map/all_to_all | solution.py:173
  147.3 1.8 join.2
  149.1 8.5 %all_gather.39 = bf16[256,128]{1,0:T(8,128)(2,1)S(1)} all-gather(bf16[128,128]{1,0:T(8,128)(2,1)} %join.2), channel_id=1, replica_groups=mesh['grp'=2,'far'=4,'near'=4,'x'=8,'c'=2] {'c'}, dimensions={0}, use_global_device_ids=true | all-gather | bytes 98304 | tf_op jit(solution)/shard_map/all_gather | solution.py:174
  158.6 3.6 %all-to-all-start.3 = ((bf16[8,2,8,1024]{3,2,1,0:T(8,128)(2,1)}), bf16[8,2,8,1024]{3,2,1,0:T(8,128)(2,1)S(1)}, u32[]{:S(2)}, u32[]{:S(2)}) async-start(bf16[8,2,8,1024]{3,2,1,0:T(8,128)(2,1)} %bitcast.65), calls=%async_computation.3 | async-start | bytes 524288 | tf_op jit(solution)/shard_map/all_to_all | solution.py:179
  162.2 12.1 %all-to-all-done.3 = bf16[8,2,8,1024]{3,2,1,0:T(8,128)(2,1)S(1)} async-done(((bf16[8,2,8,1024]{3,2,1,0:T(8,128)(2,1)}), bf16[8,2,8,1024]{3,2,1,0:T(8,128)(2,1)S(1)}, u32[]{:S(2)}, u32[]{:S(2)}) %all-to-all-start.3) | async-done | bytes 262176 | tf_op jit(solution)/shard_map/all_to_all | solution.py:179
  174.3 2.1 all-gather.1
  176.9 14.8 %all_to_all.41 = bf16[8,8,2048]{2,1,0:T(8,128)(2,1)S(1)} all-to-all(bf16[8,8,2048]{2,1,0:T(8,128)(2,1)S(1)} %broadcast_in_dim.10), channel_id=1, replica_groups=mesh['grp'=2,'far'=4,'near'=4,'x'=8,'c'=2] {'x'}, dimensions={0} | all-to-all | bytes 524288 | tf_op jit(solution)/shard_map/all_to_all | solution.py:125
  191.7 2.3 all-gather.2
  195.0 9.5 %all-to-all-start.5 = ((bf16[4,128,128]{2,1,0:T(8,128)(2,1)}), bf16[4,128,128]{2,1,0:T(8,128)(2,1)S(1)}, u32[]{:S(2)}, u32[]{:S(2)}) async-start(bf16[4,128,128]{2,1,0:T(8,128)(2,1)} %broadcast_in_dim.11), calls=%async_computation.5 | async-start | bytes 262144 | tf_op jit(solution)/shard_map/all_to_all | solution.py:125
  204.4 12.3 %all-to-all-done.5 = bf16[4,128,128]{2,1,0:T(8,128)(2,1)S(1)} async-done(((bf16[4,128,128]{2,1,0:T(8,128)(2,1)}), bf16[4,128,128]{2,1,0:T(8,128)(2,1)S(1)}, u32[]{:S(2)}, u32[]{:S(2)}) %all-to-all-start.5) | async-done | bytes 131104 | tf_op jit(solution)/shard_map/all_to_all | solution.py:125
  216.8 1.6 copy-done
  218.3 3.8 %attend.3 = bf16[4,136,128]{2,1,0:T(8,128)(2,1)S(1)} custom-call(bf16[512,128]{1,0:T(8,128)(2,1)S(1)} %bitcast.66, bf16[4096,256]{1,0:T(8,128)(2,1)S(1)} %copy-done, bf16[4096,256]{1,0:T(8,128)(2,1)S(1)} %copy-done), custom_call_target="tpu_custom_call" | custom-call | flops 1073741824 | bytes 2359296 | tf_op jit(solution)/shard_map/attend/pallas_call | solution.py:78
  222.1 18.0 %all_to_all.42.g_ref = bf16[4,136,128]{2,1,0:T(8,128)(2,1)} all-to-all(bf16[4,136,128]{2,1,0:T(8,128)(2,1)S(1)} %attend.3), channel_id=1, replica_groups=mesh['grp'=2,'far'=4,'near'=4,'x'=8,'c'=2] {'far'}, dimensions={0} | all-to-all | bytes 278528 | tf_op jit(solution)/shard_map/all_to_all | solution.py:173
  240.1 1.6 join.3
  241.7 4.3 %all_gather.45 = bf16[256,128]{1,0:T(8,128)(2,1)S(1)} all-gather(bf16[128,128]{1,0:T(8,128)(2,1)} %join.3), channel_id=1, replica_groups=mesh['grp'=2,'far'=4,'near'=4,'x'=8,'c'=2] {'c'}, dimensions={0}, use_global_device_ids=true | all-gather | bytes 98304 | tf_op jit(solution)/shard_map/all_gather | solution.py:174
  246.2 14.8 %all_to_all.43 = bf16[8,2,8,1024]{3,2,1,0:T(8,128)(2,1)S(1)} all-to-all(bf16[8,2,8,1024]{3,2,1,0:T(8,128)(2,1)S(1)} %bitcast.70), channel_id=1, replica_groups=mesh['grp'=2,'far'=4,'near'=4,'x'=8,'c'=2] {'x'}, dimensions={0} | all-to-all | bytes 524288 | tf_op jit(solution)/shard_map/all_to_all | solution.py:179
  261.1 2.1 all-gather.3
  (48 shorter events, 6.2 us)
Async XLA Ops:
  6.5 94.3 %all-gather.7.cloned.1.call-start = ((), (), s32[]{:S(2)}) async-start(), calls=%async_computation.8 | async-start | bytes 4456448 | tf_op jit(solution)/shard_map/all_gather | solution.py:148
  9.9 68.5 %copy-start.2 = (bf16[2,128,2048]{2,1,0:T(8,128)(2,1)S(1)}, bf16[2,128,2048]{2,1,0:T(8,128)(2,1)}, u32[]{:S(2)}) copy-start(bf16[2,128,2048]{2,1,0:T(8,128)(2,1)} %param.12) | copy-start | bytes 3145732
  27.0 54.0 %copy-start.3 = (bf16[2,2048,128]{2,1,0:T(8,128)(2,1)S(1)}, bf16[2,2048,128]{2,1,0:T(8,128)(2,1)}, u32[]{:S(2)}) copy-start(bf16[2,2048,128]{2,1,0:T(8,128)(2,1)} %param.11) | copy-start | bytes 3145732
  68.6 32.3 %all-to-all-start.1 = ((bf16[16,128,128]{2,1,0:T(8,128)(2,1)}), bf16[16,128,128]{2,1,0:T(8,128)(2,1)S(1)}, u32[]{:S(2)}, u32[]{:S(2)}) async-start(bf16[16,128,128]{2,1,0:T(8,128)(2,1)} %broadcast_in_dim.9), calls=%async_computation.1 | async-start | bytes 1048576 | tf_op jit(solution)/shard_map/all_to_all | solution.py:125
  78.4 5.2 %collective-permute-start = (bf16[2,128,1024]{2,1,0:T(8,128)(2,1)S(1)}, bf16[2,128,1024]{2,1,0:T(8,128)(2,1)}, u32[]{:S(2)}, u32[]{:S(2)}) collective-permute-start(bf16[2,128,1024]{2,1,0:T(8,128)(2,1)S(1)} %constant_dynamic-slice_fusion.2), channel_id=1, source_target_pairs={{0,1},{1,0},{2,3},{3,2},{4,5},{5,4},{6,7},{7,6},{8,9},{9,8},{10,11... | collective-permute-start | bytes 1572872 | tf_op jit(solution)/shard_map/ppermute | solution.py:159
  83.6 17.3 %copy-start.7 = (bf16[2048,128]{1,0:T(8,128)(2,1)S(1)}, bf16[2048,128]{1,0:T(8,128)(2,1)}, u32[]{:S(2)}) copy-start(bf16[2048,128]{1,0:T(8,128)(2,1)} %get-tuple-element.18) | copy-start | bytes 1572868
  83.6 17.3 %copy-start.8 = (bf16[2048,128]{1,0:T(8,128)(2,1)S(1)}, bf16[2048,128]{1,0:T(8,128)(2,1)}, u32[]{:S(2)}) copy-start(bf16[2048,128]{1,0:T(8,128)(2,1)} %get-tuple-element.23) | copy-start | bytes 1572868
  104.3 18.4 %copy-start.5 = (bf16[2048,128]{1,0:T(8,128)(2,1)S(1)}, bf16[2048,128]{1,0:T(8,128)(2,1)}, u32[]{:S(2)}) copy-start(bf16[2048,128]{1,0:T(8,128)(2,1)} %get-tuple-element.17) | copy-start | bytes 1572868
  104.4 18.4 %copy-start.6 = (bf16[2048,128]{1,0:T(8,128)(2,1)S(1)}, bf16[2048,128]{1,0:T(8,128)(2,1)}, u32[]{:S(2)}) copy-start(bf16[2048,128]{1,0:T(8,128)(2,1)} %get-tuple-element.24) | copy-start | bytes 1572868
  109.6 36.9 %all-to-all-start.2 = ((bf16[16,136,128]{2,1,0:T(8,128)(2,1)}), bf16[16,136,128]{2,1,0:T(8,128)(2,1)S(1)}, u32[]{:S(2)}, u32[]{:S(2)}) async-start(bf16[16,136,128]{2,1,0:T(8,128)(2,1)} %attend.2), calls=%async_computation.2 | async-start | bytes 1114112 | tf_op jit(solution)/shard_map/all_to_all | solution.py:173
  122.6 81.8 %all-gather.9.cloned.1.call-start = ((), (), s32[]{:S(2)}) async-start(), calls=%async_computation.9 | async-start | bytes 2621440 | tf_op jit(solution)/shard_map/all_gather | solution.py:154
  127.0 49.6 %copy-start.4 = (bf16[8,2048]{1,0:T(8,128)(2,1)S(1)}, bf16[8,2048]{1,0:T(8,128)(2,1)}, u32[]{:S(2)}) copy-start(bf16[8,2048]{1,0:T(8,128)(2,1)} %param.7) | copy-start | bytes 98308
  146.5 0.8 copy-start.1
  157.6 36.4 %copy-start.9 = (bf16[2,2048,128]{2,1,0:T(8,128)(2,1)S(1)}, bf16[2,2048,128]{2,1,0:T(8,128)(2,1)}, u32[]{:S(2)}) copy-start(bf16[2,2048,128]{2,1,0:T(8,128)(2,1)} %param.9) | copy-start | bytes 3145732
  158.6 15.7 %all-to-all-start.3 = ((bf16[8,2,8,1024]{3,2,1,0:T(8,128)(2,1)}), bf16[8,2,8,1024]{3,2,1,0:T(8,128)(2,1)S(1)}, u32[]{:S(2)}, u32[]{:S(2)}) async-start(bf16[8,2,8,1024]{3,2,1,0:T(8,128)(2,1)} %bitcast.65), calls=%async_computation.3 | async-start | bytes 524288 | tf_op jit(solution)/shard_map/all_to_all | solution.py:179
  195.0 21.8 %all-to-all-start.5 = ((bf16[4,128,128]{2,1,0:T(8,128)(2,1)}), bf16[4,128,128]{2,1,0:T(8,128)(2,1)S(1)}, u32[]{:S(2)}, u32[]{:S(2)}) async-start(bf16[4,128,128]{2,1,0:T(8,128)(2,1)} %broadcast_in_dim.11), calls=%async_computation.5 | async-start | bytes 262144 | tf_op jit(solution)/shard_map/all_to_all | solution.py:125
  216.8 1.6 copy-start
Sparse Core Ops, SparseCore 0:
  9.5 83.0 all-gather.6
  127.2 56.8 all-gather.8

commit v3 on v2

--- a/solution.py
+++ b/solution.py
@@ -12,11 +12,11 @@
 EPS = 1e-06
 LOG2E = 1.4426950408889634
 TP = ("x", "c")
-SP = ("far", "near")
-ROWS = ("grp", "far", "near", "x", "c")
+SP = ("far", "mid", "near")
+ROWS = ("grp", "far", "mid", "near", "x", "c")
 STATS = 8
 BLOCK = 128
-NEAR = 4
+PAIR = 2
 
 
 def split3(v):
@@ -25,37 +25,41 @@
     return hi, mid, v - hi - mid
 
 
-def attend_kernel(rows, chunk, q_ref, k_ref, v_ref, o_ref, values_ref):
-    sources = k_ref.shape[0]
+def attend_kernel(rows, chunk, q_ref, *refs):
+    held = (len(refs) - 1) // 3
+    k_refs, v_refs, o_ref, t_refs = refs[:held], refs[held : 2 * held], refs[2 * held], refs[2 * held + 1 :]
+    sources = k_refs[0].shape[0]
     scale = HEAD**-0.5 * LOG2E
     half = STATS // 2
-    values_ref[...] = jnp.transpose(v_ref[...].astype(jnp.float32)).astype(jnp.bfloat16)
+    for v_ref, t_ref in zip(v_refs, t_refs):
+        t_ref[...] = jnp.transpose(v_ref[...].astype(jnp.float32)).astype(jnp.bfloat16)
 
     def step(index, carry):
         queries = q_ref[pl.ds(pl.multiple_of(index * rows, rows), rows), :]
         peak = total = out = None
-        for at in range(0, sources, chunk):
-            scores = lax.dot_general(
-                k_ref[at : at + chunk, :],
-                queries,
-                (((1,), (1,)), ((), ())),
-                preferred_element_type=jnp.float32,
-            )
-            top = jnp.max(scores, axis=0, keepdims=True)
-            new = top if peak is None else jnp.maximum(peak, top)
-            weights = jnp.exp2((scores - new) * scale)
-            here = jnp.sum(weights, axis=0, keepdims=True)
-            part = jnp.dot(
-                values_ref[:, at : at + chunk],
-                weights.astype(jnp.bfloat16),
-                preferred_element_type=jnp.float32,
-            )
-            if peak is None:
-                total, out = here, part
-            else:
-                fade = jnp.exp2((peak - new) * scale)
-                total, out = total * fade + here, out * fade + part
-            peak = new
+        for k_ref, t_ref in zip(k_refs, t_refs):
+            for at in range(0, sources, chunk):
+                scores = lax.dot_general(
+                    k_ref[at : at + chunk, :],
+                    queries,
+                    (((1,), (1,)), ((), ())),
+                    preferred_element_type=jnp.float32,
+                )
+                top = jnp.max(scores, axis=0, keepdims=True)
+                new = top if peak is None else jnp.maximum(peak, top)
+                weights = jnp.exp2((scores - new) * scale)
+                here = jnp.sum(weights, axis=0, keepdims=True)
+                part = jnp.dot(
+                    t_ref[:, at : at + chunk],
+                    weights.astype(jnp.bfloat16),
+                    preferred_element_type=jnp.float32,
+                )
+                if peak is None:
+                    total, out = here, part
+                else:
+                    fade = jnp.exp2((peak - new) * scale)
+                    total, out = total * fade + here, out * fade + part
+                peak = new
         out = (out / total).astype(jnp.bfloat16)
         row = lax.broadcasted_iota(jnp.int32, (STATS, rows), 0)
         hi, mid, low = split3(jnp.where(row < half, peak * scale, total))
@@ -71,8 +75,8 @@
     lax.fori_loop(0, q_ref.shape[0] // rows, step, 0)
 
 
-def attend(queries, projected):
-    rows, sources = queries.shape[0], projected.shape[0]
+def attend(queries, *held):
+    rows, sources = queries.shape[0], held[0].shape[0]
     blocks = rows // BLOCK
     out = (blocks, HEAD + STATS, BLOCK)
     return pl.pallas_call(
@@ -80,20 +84,20 @@
         grid=(1,),
         in_specs=[
             pl.BlockSpec((rows, HEAD), lambda i: (0, 0)),
-            pl.BlockSpec((sources, HEAD), lambda i: (0, 0)),
-            pl.BlockSpec((sources, HEAD), lambda i: (0, 1)),
+            *(pl.BlockSpec((sources, HEAD), lambda i: (0, 0)) for _ in held),
+            *(pl.BlockSpec((sources, HEAD), lambda i: (0, 1)) for _ in held),
         ],
         out_specs=pl.BlockSpec(out, lambda i: (0, 0, 0)),
         out_shape=jax.ShapeDtypeStruct(out, jnp.bfloat16),
-        scratch_shapes=[pltpu.VMEM((HEAD, sources), jnp.bfloat16)],
+        scratch_shapes=[pltpu.VMEM((HEAD, sources), jnp.bfloat16) for _ in held],
         compiler_params=pltpu.CompilerParams(vmem_limit_bytes=32 * 2**20),
         cost_estimate=pl.CostEstimate(
-            flops=4 * rows * sources * HEAD,
-            bytes_accessed=4 * rows * HEAD + 4 * sources * HEAD,
-            transcendentals=rows * sources,
+            flops=4 * rows * sources * HEAD * len(held),
+            bytes_accessed=4 * rows * HEAD + 4 * sources * HEAD * len(held),
+            transcendentals=rows * sources * len(held),
         ),
         name="attend",
-    )(queries, projected, projected)
+    )(queries, *held, *held)
 
 
 def join_kernel(g_ref, o_ref):
@@ -146,13 +150,10 @@
     core = lax.axis_index("c")
 
     rows_here = lax.all_gather(source, TP, axis=0, tiled=True)
-    projected_source = []
-    for level in range(depth):
+
+    def keys_values(level):
         both = jnp.concatenate([w_key[level], w_value[level]], axis=1)
-        both = dot(rows_here, both).astype(jnp.bfloat16)
-        if level > 0:
-            both = lax.all_gather(both, "near", axis=0, tiled=True)
-        projected_source.append(both)
+        return dot(rows_here, both).astype(jnp.bfloat16)
 
     mine = lax.dynamic_slice_in_dim(w_out, core * side, side, 2)
     other = lax.dynamic_slice_in_dim(w_out, (1 - core) * side, side, 2)
@@ -165,11 +166,17 @@
     for level in range(depth):
         normed = normalize(stream, gains[level, 0]).astype(jnp.bfloat16)
         normed = lax.all_gather(to_all(normed, "x"), "c").reshape(block, width)
-        peers = SP if level == 0 else "far"
-        queries = to_all(dot(normed, w_query[level]).astype(jnp.bfloat16), peers)
+        queries = dot(normed, w_query[level]).astype(jnp.bfloat16)
         if level == 0:
-            queries, w_mix = lax.optimization_barrier((queries, w_mix))
-        partial = attend(queries.reshape(-1, HEAD), projected_source[level])
+            here = keys_values(level)
+            held = (here, lax.ppermute(here, "near", [(0, 1), (1, 0)]))
+            peers = ("far", "mid")
+            queries, w_mix = lax.optimization_barrier((to_all(queries, peers), w_mix))
+        else:
+            held = (lax.all_gather(keys_values(level), ("mid", "near"), axis=0, tiled=True),)
+            peers = "far"
+            queries = to_all(queries, peers)
+        partial = attend(queries.reshape(-1, HEAD), *held)
         attended = join(lax.all_to_all(partial, peers, 0, 0, tiled=True))
         pair = lax.all_gather(attended, "c", axis=0, tiled=True)
         mixed = lax.dot_general(
@@ -187,7 +194,7 @@
 
 def solution(mesh):
     split = Mesh(
-        mesh.devices.reshape(mesh.shape["grp"], mesh.shape["sp"] // NEAR, NEAR, -1, 2), ROWS
+        mesh.devices.reshape(mesh.shape["grp"], -1, PAIR, PAIR, mesh.shape["tp"] // 2, 2), ROWS
     )
     placed = (
         P(ROWS, None),

time: 272 us -> 263 us (0.967)
  starting transfers between devices: 38.5 us -> 73.8 us
  blocking collectives: 123 us -> 90.3 us
  waiting for transfers between devices: 60.4 us -> 51.9 us
    ppermute x1, starting transfers between devices: 2.59 us -> 39.1 us  [body(): other = lax.ppermute(other, 'c', [(0, 1), (1, 0)])]
    all_gather x2, blocking collectives: 41.6 us -> 9.98 us  [body(): normed = lax.all_gather(to_all(normed, 'x'), 'c').reshape(block, width)]
    all_to_all x2, waiting for transfers between devices: 28.1 us -> 0.01 us  [to_all(): return lax.all_to_all(copies, axis, 0, 0, tiled=True)]
    all_gather x1, waiting for transfers between devices: 0.01 us -> 15.9 us  [body(): rows_here = lax.all_gather(source, TP, axis=0, tiled=True)]
    ppermute x0 -> x1, waiting for transfers between devices: none -> 11.4 us  [body(): held = (here, lax.ppermute(here, 'near', [(0, 1), (1, 0)]))]
    all_to_all x1, waiting for transfers between devices: 19.4 us -> 12.5 us  [body(): attended = join(lax.all_to_all(partial, peers, 0, 0, tiled=True))]
    all_to_all x2, starting transfers between devices: 19.2 us -> 14.6 us  [to_all(): return lax.all_to_all(copies, axis, 0, 0, tiled=True)]
    ppermute x0 -> x1, starting transfers between devices: none -> 3.5 us  [body(): held = (here, lax.ppermute(here, 'near', [(0, 1), (1, 0)]))]
  transfers between devices with their start and end apart: 7 -> 8, of which waited for: 4 -> 4; matrix products, arithmetic and copies ran while one was open for 6% -> 7% of each run, Pallas kernels for 1% -> 1%
where the time goes in v3:
time: 263 us; the launch traced here: 262 us
  blocking collectives  90.3 us (34%)
  starting transfers between devices  73.8 us (28%)
  waiting for transfers between devices  51.9 us (20%)
  between operations  13.6 us (5%)
  Pallas kernels  11.6 us (4%)
  matrix products  10 us (4%)
  local copies, waits for them, and re-layouts  7.8 us (3%)
  other arithmetic  3.44 us (1%)
    ppermute x1, starting transfers between devices, body(): other = lax.ppermute(other, 'c', [(0, 1), (1, 0)])  39.1 us
    all_to_all x2, blocking collectives, to_all(): return lax.all_to_all(copies, axis, 0, 0, tiled=True)  29.6 us
    all_to_all x1, blocking collectives, body(): attended = join(lax.all_to_all(partial, peers, 0, 0, tiled=True))  17.1 us
    all_gather x1, waiting for transfers between devices, body(): rows_here = lax.all_gather(source, TP, axis=0, tiled=True)  15.9 us
    all_to_all x2, starting transfers between devices, to_all(): return lax.all_to_all(copies, axis, 0, 0, tiled=True)  14.6 us
    all_to_all x1, blocking collectives, body(): mixed = lax.all_to_all(mixed, 'x', 0, 0, tiled=True)  13.8 us
    all_gather x2, blocking collectives, body(): pair = lax.all_gather(attended, 'c', axis=0, tiled=True)  13.3 us
    all_to_all x1, waiting for transfers between devices, body(): attended = join(lax.all_to_all(partial, peers, 0, 0, tiled=True))  12.5 us
  transfers between devices with their start and end apart: 8, of which 4 were waited for; matrix products, arithmetic and copies ran while one was open for 7% of the time, Pallas kernels for 1%

profile of v3, /device:TPU:65, one launch (start us, length us, event | category | flops | bytes accessed | tf_op | source)
XLA Modules:
  0.0 262.4 jit_solution(15297013638326272354)
XLA Ops:
  7.3 0.9 fusion.18
  9.0 0.8 fusion.20
  10.6 7.9 %all-to-all-start = ((bf16[8,8,2048]{2,1,0:T(8,128)(2,1)}), bf16[8,8,2048]{2,1,0:T(8,128)(2,1)S(1)}, u32[]{:S(2)}, u32[]{:S(2)}) async-start(bf16[8,8,2048]{2,1,0:T(8,128)(2,1)} %broadcast_in_dim.8), calls=%async_computation | async-start | bytes 524288 | tf_op jit(solution)/shard_map/all_to_all | solution.py:129
  18.5 1.1 constant_dynamic-slice_fusion.2
  19.5 39.1 %collective-permute-start = (bf16[2,128,1024]{2,1,0:T(8,128)(2,1)S(1)}, bf16[2,128,1024]{2,1,0:T(8,128)(2,1)S(1)}, u32[]{:S(2)}, u32[]{:S(2)}) collective-permute-start(bf16[2,128,1024]{2,1,0:T(8,128)(2,1)S(1)} %constant_dynamic-slice_fusion.2), channel_id=1, source_target_pairs={{0,1},{1,0},{2,3},{3,2},{4,5},{5,4},{6,7},{7,6},{8,9},{9,8},{10,11... | collective-permute-start | bytes 1572872 | tf_op jit(solution)/shard_map/ppermute | solution.py:160
  58.7 1.3 slice_bitcast_fusion
  60.0 7.7 %all-gather = bf16[16,8,2048]{2,1,0:T(8,128)(2,1)S(1)} all-gather(bf16[8,8,2048]{2,1,0:T(8,128)(2,1)S(1)} %all-to-all-done), channel_id=2, replica_groups=mesh['grp'=2,'far'=4,'mid'=2,'near'=2,'x'=8,'c'=2] {'c'}, dimensions={0}, use_global_device_ids=true | all-gather | bytes 786432 | tf_op jit(solution)/shard_map/all_gather | solution.py:168
  67.7 1.4 convolution_convert_fusion.5
  69.8 6.8 %all-to-all-start.1 = ((bf16[8,128,128]{2,1,0:T(8,128)(2,1)}), bf16[8,128,128]{2,1,0:T(8,128)(2,1)S(1)}, u32[]{:S(2)}, u32[]{:S(2)}) async-start(bf16[8,128,128]{2,1,0:T(8,128)(2,1)} %broadcast_in_dim.9), calls=%async_computation.1 | async-start | bytes 524288 | tf_op jit(solution)/shard_map/all_to_all | solution.py:129
  76.6 15.9 %all-gather.7.cloned.1.call-done = bf16[1024,2048]{1,0:T(8,128)(2,1)} async-done(((bf16[64,2048]{1,0:T(8,128)(2,1)}), bf16[1024,2048]{1,0:T(8,128)(2,1)}) %all-gather.7.cloned.1.call-update) | async-done | bytes 4194320 | tf_op jit(solution)/shard_map/all_gather | solution.py:152
  92.5 3.6 %fusion.refs_0_.refs_2_ = bf16[1024,256]{1,0:T(8,128)(2,1)S(1)} fusion(bf16[1024,2048]{1,0:T(8,128)(2,1)} %all-gather.7.cloned.1.call-done, bf16[2048,128]{1,0:T(8,128)(2,1)S(1)} %copy-done.8, bf16[2048,128]{1,0:T(8,128)(2,1)} %get-tuple-element.23), kind=kOutput, calls=%fused_computation.2 | convolution fusion | flops 1076101120 | bytes 5767168 | tf_op jit(solution)/shard_map/dot_general | solution.py:141
  96.1 3.5 %collective-permute-start.1 = (bf16[1024,256]{1,0:T(8,128)(2,1)S(1)}, bf16[1024,256]{1,0:T(8,128)(2,1)S(1)}, u32[]{:S(2)}, u32[]{:S(2)}) collective-permute-start(bf16[1024,256]{1,0:T(8,128)(2,1)S(1)} %fusion.refs_0_.refs_2_), channel_id=1, source_target_pairs={{0,16},{16,0},{1,17},{17,1},{2,18},{18,2},{3,19},{19,3},{4,20},{20... | collective-permute-start | bytes 1572872 | tf_op jit(solution)/shard_map/ppermute | solution.py:172
  100.0 11.4 %collective-permute-done.1.refs_1_.refs_3_ = bf16[1024,256]{1,0:T(8,128)(2,1)S(1)} collective-permute-done((bf16[1024,256]{1,0:T(8,128)(2,1)S(1)}, bf16[1024,256]{1,0:T(8,128)(2,1)S(1)}, u32[]{:S(2)}, u32[]{:S(2)}) %collective-permute-start.1) | collective-permute-done | bytes 524320 | tf_op jit(solution)/shard_map/ppermute | solution.py:172
  111.5 4.7 %attend.2 = bf16[8,136,128]{2,1,0:T(8,128)(2,1)} custom-call(bf16[1024,128]{1,0:T(8,128)(2,1)S(1)} %bitcast.67, bf16[1024,256]{1,0:T(8,128)(2,1)S(1)} %fusion.refs_0_.refs_2_, bf16[1024,256]{1,0:T(8,128)(2,1)S(1)} %collective-permute-done.1.refs_1_.refs_3_, bf16[1024,256]{1,0:T(8,128)(2,1)S(1)} %fusion.refs_0_.refs_2_, ...), custom_call_target="tpu_custom_call" | custom-call | flops 1073741824 | bytes 1572864 | tf_op jit(solution)/shard_map/attend/pallas_call | solution.py:82
  116.1 12.5 %all-to-all-start.2 = ((bf16[8,136,128]{2,1,0:T(8,128)(2,1)}), bf16[8,136,128]{2,1,0:T(8,128)(2,1)S(1)}, u32[]{:S(2)}, u32[]{:S(2)}) async-start(bf16[8,136,128]{2,1,0:T(8,128)(2,1)} %attend.2), calls=%async_computation.2 | async-start | bytes 557056 | tf_op jit(solution)/shard_map/all_to_all | solution.py:180
  128.7 4.2 %fusion.1 = bf16[1024,256]{1,0:T(8,128)(2,1)} fusion(bf16[1024,2048]{1,0:T(8,128)(2,1)} %all-gather.7.cloned.1.call-done, bf16[2048,128]{1,0:T(8,128)(2,1)S(1)} %copy-done.6, bf16[2048,128]{1,0:T(8,128)(2,1)S(1)} %copy-done.7), kind=kOutput, calls=%fused_computation.3 | convolution fusion | flops 1076101120 | bytes 5767168 | tf_op jit(solution)/shard_map/dot_general | solution.py:141
  133.0 12.5 %all-to-all-done.2.g_ref = bf16[8,136,128]{2,1,0:T(8,128)(2,1)S(1)} async-done(((bf16[8,136,128]{2,1,0:T(8,128)(2,1)}), bf16[8,136,128]{2,1,0:T(8,128)(2,1)S(1)}, u32[]{:S(2)}, u32[]{:S(2)}) %all-to-all-start.2) | async-done | bytes 278560 | tf_op jit(solution)/shard_map/all_to_all | solution.py:180
  146.2 1.7 join.2
  147.9 7.6 %all_gather.39 = bf16[256,128]{1,0:T(8,128)(2,1)S(1)} all-gather(bf16[128,128]{1,0:T(8,128)(2,1)} %join.2), channel_id=1, replica_groups=mesh['grp'=2,'far'=4,'mid'=2,'near'=2,'x'=8,'c'=2] {'c'}, dimensions={0}, use_global_device_ids=true | all-gather | bytes 98304 | tf_op jit(solution)/shard_map/all_gather | solution.py:181
  156.5 3.9 %all-to-all-start.3 = ((bf16[8,2,8,1024]{3,2,1,0:T(8,128)(2,1)}), bf16[8,2,8,1024]{3,2,1,0:T(8,128)(2,1)S(1)}, u32[]{:S(2)}, u32[]{:S(2)}) async-start(bf16[8,2,8,1024]{3,2,1,0:T(8,128)(2,1)} %bitcast.65), calls=%async_computation.3 | async-start | bytes 524288 | tf_op jit(solution)/shard_map/all_to_all | solution.py:186
  160.4 11.2 %all-to-all-done.3 = bf16[8,2,8,1024]{3,2,1,0:T(8,128)(2,1)S(1)} async-done(((bf16[8,2,8,1024]{3,2,1,0:T(8,128)(2,1)}), bf16[8,2,8,1024]{3,2,1,0:T(8,128)(2,1)S(1)}, u32[]{:S(2)}, u32[]{:S(2)}) %all-to-all-start.3) | async-done | bytes 262176 | tf_op jit(solution)/shard_map/all_to_all | solution.py:186
  171.6 3.2 %all-gather.1 = f32[4,8,1024]{2,1,0:T(8,128)S(1)} all-gather(f32[2,8,1024]{2,1,0:T(8,128)S(1)} %convert_reduce_fusion.1), channel_id=3, replica_groups=mesh['grp'=2,'far'=4,'mid'=2,'near'=2,'x'=8,'c'=2] {'c'}, dimensions={0}, use_global_device_ids=true | all-gather | bytes 196608 | tf_op jit(solution)/shard_map/all_gather | solution.py:188
  175.4 14.8 %all_to_all.40 = bf16[8,8,2048]{2,1,0:T(8,128)(2,1)S(1)} all-to-all(bf16[8,8,2048]{2,1,0:T(8,128)(2,1)S(1)} %broadcast_in_dim.10), channel_id=1, replica_groups=mesh['grp'=2,'far'=4,'mid'=2,'near'=2,'x'=8,'c'=2] {'x'}, dimensions={0} | all-to-all | bytes 524288 | tf_op jit(solution)/shard_map/all_to_all | solution.py:129
  190.1 2.3 all-gather.2
  192.8 14.8 %all_to_all.41 = bf16[4,128,128]{2,1,0:T(8,128)(2,1)S(1)} all-to-all(bf16[4,128,128]{2,1,0:T(8,128)(2,1)S(1)} %broadcast_in_dim.11), channel_id=1, replica_groups=mesh['grp'=2,'far'=4,'mid'=2,'near'=2,'x'=8,'c'=2] {'far'}, dimensions={0} | all-to-all | bytes 262144 | tf_op jit(solution)/shard_map/all_to_all | solution.py:129
  207.6 1.6 copy-done
  209.2 3.7 %attend.3 = bf16[4,136,128]{2,1,0:T(8,128)(2,1)S(1)} custom-call(bf16[512,128]{1,0:T(8,128)(2,1)S(1)} %bitcast.66, bf16[4096,256]{1,0:T(8,128)(2,1)S(1)} %copy-done, bf16[4096,256]{1,0:T(8,128)(2,1)S(1)} %copy-done), custom_call_target="tpu_custom_call" | custom-call | flops 1073741824 | bytes 2359296 | tf_op jit(solution)/shard_map/attend/pallas_call | solution.py:82
  212.9 17.1 %all_to_all.42.g_ref = bf16[4,136,128]{2,1,0:T(8,128)(2,1)} all-to-all(bf16[4,136,128]{2,1,0:T(8,128)(2,1)S(1)} %attend.3), channel_id=1, replica_groups=mesh['grp'=2,'far'=4,'mid'=2,'near'=2,'x'=8,'c'=2] {'far'}, dimensions={0} | all-to-all | bytes 278528 | tf_op jit(solution)/shard_map/all_to_all | solution.py:180
  230.0 1.6 join.3
  231.6 5.7 %all_gather.45 = bf16[256,128]{1,0:T(8,128)(2,1)S(1)} all-gather(bf16[128,128]{1,0:T(8,128)(2,1)} %join.3), channel_id=1, replica_groups=mesh['grp'=2,'far'=4,'mid'=2,'near'=2,'x'=8,'c'=2] {'c'}, dimensions={0}, use_global_device_ids=true | all-gather | bytes 98304 | tf_op jit(solution)/shard_map/all_gather | solution.py:181
  237.6 13.8 %all_to_all.43 = bf16[8,2,8,1024]{3,2,1,0:T(8,128)(2,1)S(1)} all-to-all(bf16[8,2,8,1024]{3,2,1,0:T(8,128)(2,1)S(1)} %bitcast.70), channel_id=1, replica_groups=mesh['grp'=2,'far'=4,'mid'=2,'near'=2,'x'=8,'c'=2] {'x'}, dimensions={0} | all-to-all | bytes 524288 | tf_op jit(solution)/shard_map/all_to_all | solution.py:186
  251.4 3.2 %all-gather.3 = f32[4,8,1024]{2,1,0:T(8,128)S(1)} all-gather(f32[2,8,1024]{2,1,0:T(8,128)S(1)} %convert_reduce_fusion), channel_id=5, replica_groups=mesh['grp'=2,'far'=4,'mid'=2,'near'=2,'x'=8,'c'=2] {'c'}, dimensions={0}, use_global_device_ids=true | all-gather | bytes 196608 | tf_op jit(solution)/shard_map/all_gather | solution.py:188
  (50 shorter events, 7.2 us)
Async XLA Ops:
  6.5 52.1 %copy-start.3 = (bf16[2,2048,128]{2,1,0:T(8,128)(2,1)S(1)}, bf16[2,2048,128]{2,1,0:T(8,128)(2,1)}, u32[]{:S(2)}) copy-start(bf16[2,2048,128]{2,1,0:T(8,128)(2,1)} %param.11) | copy-start | bytes 3145732
  6.5 52.2 %copy-start.4 = (bf16[2,2048,128]{2,1,0:T(8,128)(2,1)S(1)}, bf16[2,2048,128]{2,1,0:T(8,128)(2,1)}, u32[]{:S(2)}) copy-start(bf16[2,2048,128]{2,1,0:T(8,128)(2,1)} %param.10) | copy-start | bytes 3145732
  6.6 85.9 %all-gather.7.cloned.1.call-start = ((), (), s32[]{:S(2)}) async-start(), calls=%async_computation.8 | async-start | bytes 4456448 | tf_op jit(solution)/shard_map/all_gather | solution.py:152
  10.6 49.5 %all-to-all-start = ((bf16[8,8,2048]{2,1,0:T(8,128)(2,1)}), bf16[8,8,2048]{2,1,0:T(8,128)(2,1)S(1)}, u32[]{:S(2)}, u32[]{:S(2)}) async-start(bf16[8,8,2048]{2,1,0:T(8,128)(2,1)} %broadcast_in_dim.8), calls=%async_computation | async-start | bytes 524288 | tf_op jit(solution)/shard_map/all_to_all | solution.py:129
  19.5 80.1 %collective-permute-start = (bf16[2,128,1024]{2,1,0:T(8,128)(2,1)S(1)}, bf16[2,128,1024]{2,1,0:T(8,128)(2,1)S(1)}, u32[]{:S(2)}, u32[]{:S(2)}) collective-permute-start(bf16[2,128,1024]{2,1,0:T(8,128)(2,1)S(1)} %constant_dynamic-slice_fusion.2), channel_id=1, source_target_pairs={{0,1},{1,0},{2,3},{3,2},{4,5},{5,4},{6,7},{7,6},{8,9},{9,8},{10,11... | collective-permute-start | bytes 1572872 | tf_op jit(solution)/shard_map/ppermute | solution.py:160
  60.0 32.4 %copy-start.8 = (bf16[2048,128]{1,0:T(8,128)(2,1)S(1)}, bf16[2048,128]{1,0:T(8,128)(2,1)}, u32[]{:S(2)}) copy-start(bf16[2048,128]{1,0:T(8,128)(2,1)} %get-tuple-element.18) | copy-start | bytes 1572868
  69.8 30.2 %all-to-all-start.1 = ((bf16[8,128,128]{2,1,0:T(8,128)(2,1)}), bf16[8,128,128]{2,1,0:T(8,128)(2,1)S(1)}, u32[]{:S(2)}, u32[]{:S(2)}) async-start(bf16[8,128,128]{2,1,0:T(8,128)(2,1)} %broadcast_in_dim.9), calls=%async_computation.1 | async-start | bytes 524288 | tf_op jit(solution)/shard_map/all_to_all | solution.py:129
  92.5 7.2 %copy-start.2 = (bf16[2,128,2048]{2,1,0:T(8,128)(2,1)S(1)}, bf16[2,128,2048]{2,1,0:T(8,128)(2,1)}, u32[]{:S(2)}) copy-start(bf16[2,128,2048]{2,1,0:T(8,128)(2,1)} %param.12) | copy-start | bytes 3145732
  96.1 15.3 %collective-permute-start.1 = (bf16[1024,256]{1,0:T(8,128)(2,1)S(1)}, bf16[1024,256]{1,0:T(8,128)(2,1)S(1)}, u32[]{:S(2)}, u32[]{:S(2)}) collective-permute-start(bf16[1024,256]{1,0:T(8,128)(2,1)S(1)} %fusion.refs_0_.refs_2_), channel_id=1, source_target_pairs={{0,16},{16,0},{1,17},{17,1},{2,18},{18,2},{3,19},{19,3},{4,20},{20... | collective-permute-start | bytes 1572872 | tf_op jit(solution)/shard_map/ppermute | solution.py:172
  111.4 17.2 %copy-start.6 = (bf16[2048,128]{1,0:T(8,128)(2,1)S(1)}, bf16[2048,128]{1,0:T(8,128)(2,1)}, u32[]{:S(2)}) copy-start(bf16[2048,128]{1,0:T(8,128)(2,1)} %get-tuple-element.17) | copy-start | bytes 1572868
  111.4 17.3 %copy-start.7 = (bf16[2048,128]{1,0:T(8,128)(2,1)S(1)}, bf16[2048,128]{1,0:T(8,128)(2,1)}, u32[]{:S(2)}) copy-start(bf16[2048,128]{1,0:T(8,128)(2,1)} %get-tuple-element.24) | copy-start | bytes 1572868
  116.1 29.4 %all-to-all-start.2 = ((bf16[8,136,128]{2,1,0:T(8,128)(2,1)}), bf16[8,136,128]{2,1,0:T(8,128)(2,1)S(1)}, u32[]{:S(2)}, u32[]{:S(2)}) async-start(bf16[8,136,128]{2,1,0:T(8,128)(2,1)} %attend.2), calls=%async_computation.2 | async-start | bytes 557056 | tf_op jit(solution)/shard_map/all_to_all | solution.py:180
  128.6 78.9 %all-gather.9.cloned.1.call-start = ((), (), s32[]{:S(2)}) async-start(), calls=%async_computation.9 | async-start | bytes 2621440 | tf_op jit(solution)/shard_map/all_gather | solution.py:176
  132.9 42.1 %copy-start.5 = (bf16[8,2048]{1,0:T(8,128)(2,1)S(1)}, bf16[8,2048]{1,0:T(8,128)(2,1)}, u32[]{:S(2)}) copy-start(bf16[8,2048]{1,0:T(8,128)(2,1)} %param.7) | copy-start | bytes 98308
  145.5 0.7 copy-start.1
  155.5 37.0 %copy-start.9 = (bf16[2,2048,128]{2,1,0:T(8,128)(2,1)S(1)}, bf16[2,2048,128]{2,1,0:T(8,128)(2,1)}, u32[]{:S(2)}) copy-start(bf16[2,2048,128]{2,1,0:T(8,128)(2,1)} %param.9) | copy-start | bytes 3145732
  156.5 15.1 %all-to-all-start.3 = ((bf16[8,2,8,1024]{3,2,1,0:T(8,128)(2,1)}), bf16[8,2,8,1024]{3,2,1,0:T(8,128)(2,1)S(1)}, u32[]{:S(2)}, u32[]{:S(2)}) async-start(bf16[8,2,8,1024]{3,2,1,0:T(8,128)(2,1)} %bitcast.65), calls=%async_computation.3 | async-start | bytes 524288 | tf_op jit(solution)/shard_map/all_to_all | solution.py:186
  207.6 1.6 copy-start
Sparse Core Ops, SparseCore 0:
  9.5 82.9 all-gather.6
  133.1 55.1 all-gather.8

commit v4 on v3

--- a/solution.py
+++ b/solution.py
@@ -17,6 +17,7 @@
 STATS = 8
 BLOCK = 128
 PAIR = 2
+VMEM = pl.BlockSpec(memory_space=pltpu.VMEM)
 
 
 def split3(v):
@@ -26,13 +27,13 @@
 
 
 def attend_kernel(rows, chunk, q_ref, *refs):
-    held = (len(refs) - 1) // 3
-    k_refs, v_refs, o_ref, t_refs = refs[:held], refs[held : 2 * held], refs[2 * held], refs[2 * held + 1 :]
+    held = (len(refs) - 1) // 2
+    k_refs, o_ref, t_refs = refs[:held], refs[held], refs[held + 1 :]
     sources = k_refs[0].shape[0]
     scale = HEAD**-0.5 * LOG2E
     half = STATS // 2
-    for v_ref, t_ref in zip(v_refs, t_refs):
-        t_ref[...] = jnp.transpose(v_ref[...].astype(jnp.float32)).astype(jnp.bfloat16)
+    for k_ref, t_ref in zip(k_refs, t_refs):
+        t_ref[...] = jnp.transpose(k_ref[:, HEAD:].astype(jnp.float32)).astype(jnp.bfloat16)
 
     def step(index, carry):
         queries = q_ref[pl.ds(pl.multiple_of(index * rows, rows), rows), :]
@@ -40,7 +41,7 @@
         for k_ref, t_ref in zip(k_refs, t_refs):
             for at in range(0, sources, chunk):
                 scores = lax.dot_general(
-                    k_ref[at : at + chunk, :],
+                    k_ref[at : at + chunk, :HEAD],
                     queries,
                     (((1,), (1,)), ((), ())),
                     preferred_element_type=jnp.float32,
@@ -81,13 +82,8 @@
     out = (blocks, HEAD + STATS, BLOCK)
     return pl.pallas_call(
         functools.partial(attend_kernel, min(rows, 512), min(sources, 1024)),
-        grid=(1,),
-        in_specs=[
-            pl.BlockSpec((rows, HEAD), lambda i: (0, 0)),
-            *(pl.BlockSpec((sources, HEAD), lambda i: (0, 0)) for _ in held),
-            *(pl.BlockSpec((sources, HEAD), lambda i: (0, 1)) for _ in held),
-        ],
-        out_specs=pl.BlockSpec(out, lambda i: (0, 0, 0)),
+        in_specs=[VMEM] * (1 + len(held)),
+        out_specs=VMEM,
         out_shape=jax.ShapeDtypeStruct(out, jnp.bfloat16),
         scratch_shapes=[pltpu.VMEM((HEAD, sources), jnp.bfloat16) for _ in held],
         compiler_params=pltpu.CompilerParams(vmem_limit_bytes=32 * 2**20),
@@ -97,7 +93,7 @@
             transcendentals=rows * sources * len(held),
         ),
         name="attend",
-    )(queries, *held, *held)
+    )(queries, *held)
 
 
 def join_kernel(g_ref, o_ref):
@@ -110,13 +106,17 @@
     joined = jnp.zeros((HEAD, BLOCK), jnp.float32)
     for part in range(g_ref.shape[0]):
         joined += share[part : part + 1] * g_ref[part, :HEAD, :].astype(jnp.float32)
-    o_ref[...] = joined.astype(jnp.bfloat16)
-
-
-def join(gathered):
+    joined = jnp.transpose(joined).astype(jnp.bfloat16)
+    for copy in range(o_ref.shape[0]):
+        o_ref[copy] = joined
+
+
+def join(gathered, copies):
     return pl.pallas_call(
         join_kernel,
-        out_shape=jax.ShapeDtypeStruct((HEAD, BLOCK), jnp.bfloat16),
+        in_specs=[VMEM],
+        out_specs=VMEM,
+        out_shape=jax.ShapeDtypeStruct((copies, BLOCK, HEAD), jnp.bfloat16),
         cost_estimate=pl.CostEstimate(
             flops=2 * gathered.size, bytes_accessed=2 * gathered.size, transcendentals=0
         ),
@@ -124,12 +124,7 @@
     )(gathered)
 
 
-def to_all(block, axis):
-    copies = jnp.broadcast_to(block[None], (lax.axis_size(axis), *block.shape))
-    return lax.all_to_all(copies, axis, 0, 0, tiled=True)
-
-
-def normalize(row_block, gain_row):
+def scaled(row_block, gain_row):
     return (
         row_block
         * lax.rsqrt(jnp.mean(row_block * row_block, axis=-1, keepdims=True) + EPS)
@@ -137,8 +132,93 @@
     )
 
 
+def query_kernel(level, stream_ref, mixed_ref, gains_ref, w_ref, q_ref, out_ref):
+    stream = stream_ref[...].astype(jnp.float32)
+    if mixed_ref is not None:
+        cores = mixed_ref.shape[0]
+        projected = jnp.concatenate([mixed_ref[k] for k in range(cores)], axis=1)
+        stream = stream + scaled(projected.astype(jnp.float32), gains_ref[level - 1, 1:2, :])
+        out_ref[...] = stream
+    normed = scaled(stream, gains_ref[level, 0:1, :]).astype(jnp.bfloat16)
+    queries = jnp.dot(normed, w_ref[level], preferred_element_type=jnp.float32).astype(jnp.bfloat16)
+    for copy in range(q_ref.shape[0]):
+        q_ref[copy] = queries
+
+
+def query(level, stream, mixed, gains, w_query, copies):
+    q_shape = jax.ShapeDtypeStruct((copies, stream.shape[0], HEAD), jnp.bfloat16)
+    cost = pl.CostEstimate(
+        flops=2 * stream.size * HEAD, bytes_accessed=8 * stream.size, transcendentals=0
+    )
+    params = pltpu.CompilerParams(vmem_limit_bytes=32 * 2**20)
+    if mixed is None:
+
+        def first(stream_ref, gains_ref, w_ref, q_ref):
+            query_kernel(level, stream_ref, None, gains_ref, w_ref, q_ref, None)
+
+        queries = pl.pallas_call(
+            first,
+            in_specs=[VMEM] * 3,
+            out_specs=VMEM,
+            out_shape=q_shape,
+            cost_estimate=cost,
+            compiler_params=params,
+            name="query",
+        )(stream, gains, w_query)
+        return queries, stream
+    return pl.pallas_call(
+        functools.partial(query_kernel, level),
+        in_specs=[VMEM] * 4,
+        out_specs=(VMEM, VMEM),
+        out_shape=(q_shape, jax.ShapeDtypeStruct(stream.shape, jnp.float32)),
+        cost_estimate=cost,
+        compiler_params=params,
+        name="query",
+    )(stream, mixed, gains, w_query)
+
+
+def mix_kernel(heads_ref, w_ref, o_ref):
+    cores, chips, rows, _ = heads_ref.shape
+    total = jnp.zeros((rows, w_ref.shape[2]), jnp.float32)
+    for chip in range(chips):
+        pair = jnp.concatenate([heads_ref[core, chip] for core in range(cores)], axis=1)
+        total += jnp.dot(pair, w_ref[chip], preferred_element_type=jnp.float32)
+    total = total.astype(jnp.bfloat16)
+    if len(o_ref.shape) == 2:
+        o_ref[...] = total
+    else:
+        own = o_ref.shape[2]
+        for chip in range(o_ref.shape[0]):
+            for core in range(cores):
+                at = (core * o_ref.shape[0] + chip) * own
+                o_ref[chip, core] = total[at : at + own]
+
+
+def mix(heads, weights, out):
+    return pl.pallas_call(
+        mix_kernel,
+        in_specs=[VMEM, VMEM],
+        out_specs=VMEM,
+        out_shape=jax.ShapeDtypeStruct(out, jnp.bfloat16),
+        cost_estimate=pl.CostEstimate(
+            flops=2 * heads.size * weights.shape[2], bytes_accessed=2 * weights.size, transcendentals=0
+        ),
+        compiler_params=pltpu.CompilerParams(vmem_limit_bytes=32 * 2**20),
+        name="mix",
+    )(heads, weights)
+
+
+def shifted(block, by):
+    count = lax.axis_size(SP)
+    return lax.ppermute(block, SP, [(k, (k + by) % count) for k in range(count)])
+
+
 def dot(a, b):
     return jnp.dot(a, b, preferred_element_type=jnp.float32)
+
+
+def spread(copies, axis):
+    return lax.all_to_all(copies, axis, 0, 0, tiled=True)
 
 
 def body(target, source, w_query, w_key, w_value, w_out, gains):
@@ -158,37 +238,40 @@
     mine = lax.dynamic_slice_in_dim(w_out, core * side, side, 2)
     other = lax.dynamic_slice_in_dim(w_out, (1 - core) * side, side, 2)
     other = lax.ppermute(other, "c", [(0, 1), (1, 0)])
-    w_mix = jnp.concatenate(
-        [jnp.where(core == 0, mine, other), jnp.where(core == 0, other, mine)], axis=1
-    )
-
-    stream = target.astype(jnp.float32)
+    first, second = jnp.where(core == 0, mine, other), jnp.where(core == 0, other, mine)
+    w_mix = [jnp.concatenate([first[k], second[k]], axis=0) for k in range(depth)]
+
+    stream = spread(jnp.broadcast_to(target[None], (chips, *target.shape)), "x")
+    stream = lax.all_gather(stream, "c").reshape(block, width)
+    mixed = None
     for level in range(depth):
-        normed = normalize(stream, gains[level, 0]).astype(jnp.bfloat16)
-        normed = lax.all_gather(to_all(normed, "x"), "c").reshape(block, width)
-        queries = dot(normed, w_query[level]).astype(jnp.bfloat16)
+        last = level == depth - 1
+        peers = ("far", "mid") if level == 0 else ("far",)
+        queries, stream = query(level, stream, mixed, gains, w_query, lax.axis_size(peers))
+        queries = spread(queries, peers)
         if level == 0:
             here = keys_values(level)
             held = (here, lax.ppermute(here, "near", [(0, 1), (1, 0)]))
-            peers = ("far", "mid")
-            queries, w_mix = lax.optimization_barrier((to_all(queries, peers), w_mix))
+        partial = attend(queries.reshape(-1, HEAD), *held)
+        attended = join(spread(partial, peers), 1 if last else chips)
+        if not last:
+            here = keys_values(level + 1)
+            attended, here = lax.optimization_barrier((attended, here))
+            above = shifted(here, -1)
+            held = (here, shifted(here, 1), above, shifted(above, -1))
+            w_whole = lax.all_gather(w_mix[level], "x")
+            heads = lax.all_gather(spread(attended, "x"), "c")
+            mixed = lax.all_gather(mix(heads, w_whole, (block, side)), "c")
         else:
-            held = (lax.all_gather(keys_values(level), ("mid", "near"), axis=0, tiled=True),)
-            peers = "far"
-            queries = to_all(queries, peers)
-        partial = attend(queries.reshape(-1, HEAD), *held)
-        attended = join(lax.all_to_all(partial, peers, 0, 0, tiled=True))
-        pair = lax.all_gather(attended, "c", axis=0, tiled=True)
-        mixed = lax.dot_general(
-            pair, w_mix[level], (((0,), (0,)), ((), ())), preferred_element_type=jnp.float32
-        ).astype(jnp.bfloat16)
-        mixed = mixed.reshape(cores, chips, own, side).transpose(1, 0, 2, 3)
-        mixed = lax.all_to_all(mixed, "x", 0, 0, tiled=True)
-        mixed = jnp.sum(mixed.astype(jnp.float32), axis=0)
-        mixed = lax.all_gather(mixed, "c")
-        mixed = lax.dynamic_index_in_dim(mixed, core, 1, keepdims=False)
-        projected = mixed.transpose(1, 0, 2).reshape(own, width)
-        stream = stream + normalize(projected, gains[level, 1])
+            heads = lax.all_gather(attended, "c")
+            mixed = mix(heads, w_mix[level][None], (chips, cores, own, side))
+            mixed = jnp.sum(spread(mixed, "x").astype(jnp.float32), axis=0)
+            mixed = lax.all_gather(mixed, "c")
+            mixed = lax.dynamic_index_in_dim(mixed, core, 1, keepdims=False)
+            projected = mixed.transpose(1, 0, 2).reshape(own, width)
+            at = (core * chips + lax.axis_index("x")) * own
+            stream = lax.dynamic_slice_in_dim(stream, at, own, 0)
+            stream = stream + scaled(projected, gains[level, 1])
     return stream.astype(jnp.bfloat16)
 
 

time: 263 us -> 258 us (0.981)
  blocking collectives: 90.3 us -> 23.7 us
  waiting for transfers between devices: 51.9 us -> 94.7 us
  starting transfers between devices: 73.8 us -> 87.1 us
  Pallas kernels: 11.6 us -> 17.8 us
    all_to_all x4 -> x0, blocking collectives: 60.5 us -> none  [the longest x2 29.6 us: to_all(): return lax.all_to_all(copies, axis, 0, 0, tiled=True)]
    all_to_all x4 -> x7, waiting for transfers between devices: 23.7 us -> 65.6 us  [spread(): return lax.all_to_all(copies, axis, 0, 0, tiled=True)]
    ppermute x0 -> x3, starting transfers between devices: none -> 7.42 us  [shifted(): lax.ppermute(block, SP, [(k, (k + by) % count) for k in range(count)])]
    pallas_call x2 -> x6, Pallas kernels: 3.23 us -> 7.64 us  [the longest x2 3.49 us: join(): pl.pallas_call(join_kernel, in_specs=[VMEM], out_specs=VMEM, out_shape=ja...]
    all_gather x2 -> x1, blocking collectives: 6.47 us -> 2.1 us  [body(): mixed = lax.all_gather(mixed, 'c')]
    ppermute x1, starting transfers between devices: 39.1 us -> 43.4 us  [body(): other = lax.ppermute(other, 'c', [(0, 1), (1, 0)])]
    all_to_all x4 -> x7, starting transfers between devices: 31.1 us -> 34.3 us  [spread(): return lax.all_to_all(copies, axis, 0, 0, tiled=True)]
    dot_general x4 -> x2, matrix products: 9.52 us -> 8.27 us  [dot(): return jnp.dot(a, b, preferred_element_type=jnp.float32)]
  transfers between devices with their start and end apart: 8 -> 14, of which waited for: 4 -> 9; matrix products, arithmetic and copies ran while one was open for 7% -> 6% of each run, Pallas kernels for 1% -> 4%
where the time goes in v4:
time: 258 us; the launch traced here: 257 us
  waiting for transfers between devices  94.7 us (37%)
  starting transfers between devices  87.1 us (34%)
  blocking collectives  23.7 us (9%)
  Pallas kernels  17.8 us (7%)
  between operations  13.6 us (5%)
  matrix products  8.27 us (3%)
  local copies, waits for them, and re-layouts  7.59 us (3%)
  other arithmetic  4.04 us (2%)
    all_to_all x7, waiting for transfers between devices, spread(): return lax.all_to_all(copies, axis, 0, 0, tiled=True)  65.6 us
    ppermute x1, starting transfers between devices, body(): other = lax.ppermute(other, 'c', [(0, 1), (1, 0)])  43.4 us
    all_to_all x7, starting transfers between devices, spread(): return lax.all_to_all(copies, axis, 0, 0, tiled=True)  34.3 us
    all_gather x1, waiting for transfers between devices, body(): rows_here = lax.all_gather(source, TP, axis=0, tiled=True)  13.5 us
    ppermute x1, waiting for transfers between devices, body(): held = (here, lax.ppermute(here, 'near', [(0, 1), (1, 0)]))  13.3 us
    pallas_call x2, Pallas kernels, attend(): pl.pallas_call(functools.partial(attend_kernel, min(rows, 512), min(sourc...  10.2 us
    all_gather x1, blocking collectives, body(): heads = lax.all_gather(spread(attended, 'x'), 'c')  8.98 us
    dot_general x2, matrix products, dot(): return jnp.dot(a, b, preferred_element_type=jnp.float32)  8.27 us
  transfers between devices with their start and end apart: 14, of which 9 were waited for; matrix products, arithmetic and copies ran while one was open for 6% of the time, Pallas kernels for 4%

profile of v4, /device:TPU:65, one launch (start us, length us, event | category | flops | bytes accessed | tf_op | source)
XLA Modules:
  0.0 256.8 jit_solution(6192137092601082729)
XLA Ops:
  8.5 43.4 %collective-permute-start.1 = (bf16[2,128,1024]{2,1,0:T(8,128)(2,1)S(1)}, bf16[2,128,1024]{2,1,0:T(8,128)(2,1)S(1)}, u32[]{:S(2)}, u32[]{:S(2)}) collective-permute-start(bf16[2,128,1024]{2,1,0:T(8,128)(2,1)S(1)} %constant_dynamic-slice_fusion.1), channel_id=1, source_target_pairs={{0,1},{1,0},{2,3},{3,2},{4,5},{5,4},{6,7},{7,6},{8,9},{9,8},{10,11... | collective-permute-start | bytes 1572872 | tf_op jit(solution)/shard_map/ppermute | solution.py:240
  57.2 3.6 %all-to-all-start = ((bf16[8,8,2048]{2,1,0:T(8,128)(2,1)}), bf16[8,8,2048]{2,1,0:T(8,128)(2,1)S(1)}, u32[]{:S(2)}, u32[]{:S(2)}) async-start(bf16[8,8,2048]{2,1,0:T(8,128)(2,1)} %broadcast_in_dim.4), calls=%async_computation | async-start | bytes 524288 | tf_op jit(solution)/shard_map/all_to_all | solution.py:221
  62.2 13.2 %all-to-all-done = bf16[8,8,2048]{2,1,0:T(8,128)(2,1)S(1)} async-done(((bf16[8,8,2048]{2,1,0:T(8,128)(2,1)}), bf16[8,8,2048]{2,1,0:T(8,128)(2,1)S(1)}, u32[]{:S(2)}, u32[]{:S(2)}) %all-to-all-start) | async-done | bytes 262176 | tf_op jit(solution)/shard_map/all_to_all | solution.py:221
  75.4 2.7 %all-gather = bf16[16,8,2048]{2,1,0:T(8,128)(2,1)S(1)} all-gather(bf16[8,8,2048]{2,1,0:T(8,128)(2,1)S(1)} %all-to-all-done), channel_id=2, replica_groups=mesh['grp'=2,'far'=4,'mid'=2,'near'=2,'x'=8,'c'=2] {'c'}, dimensions={0}, use_global_device_ids=true | all-gather | bytes 786432 | tf_op jit(solution)/shard_map/all_gather | solution.py:245
  79.2 4.2 %all-to-all-start.1 = ((bf16[8,128,128]{2,1,0:T(8,128)(2,1)}), bf16[8,128,128]{2,1,0:T(8,128)(2,1)S(1)}, u32[]{:S(2)}, u32[]{:S(2)}) async-start(bf16[8,128,128]{2,1,0:T(8,128)(2,1)} %query.2), calls=%async_computation.1 | async-start | bytes 524288 | tf_op jit(solution)/shard_map/all_to_all | solution.py:221
  83.4 13.5 %all-gather.9.cloned.1.call-done = bf16[1024,2048]{1,0:T(8,128)(2,1)} async-done(((bf16[64,2048]{1,0:T(8,128)(2,1)}), bf16[1024,2048]{1,0:T(8,128)(2,1)}) %all-gather.9.cloned.1.call-update) | async-done | bytes 4194320 | tf_op jit(solution)/shard_map/all_gather | solution.py:232
  97.0 3.7 %fusion.refs_0_ = bf16[1024,256]{1,0:T(8,128)(2,1)S(1)} fusion(bf16[1024,2048]{1,0:T(8,128)(2,1)} %all-gather.9.cloned.1.call-done, bf16[2048,128]{1,0:T(8,128)(2,1)} %get-tuple-element.20, bf16[2048,128]{1,0:T(8,128)(2,1)} %get-tuple-element.25), kind=kOutput, calls=%fused_computation.2 | convolution fusion | flops 1076101120 | bytes 5767168 | tf_op jit(solution)/shard_map/dot_general | solution.py:217
  100.7 2.0 collective-permute-start
  102.6 13.3 %collective-permute-done.refs_1_ = bf16[1024,256]{1,0:T(8,128)(2,1)S(1)} collective-permute-done((bf16[1024,256]{1,0:T(8,128)(2,1)S(1)}, bf16[1024,256]{1,0:T(8,128)(2,1)S(1)}, u32[]{:S(2)}, u32[]{:S(2)}) %collective-permute-start) | collective-permute-done | bytes 524320 | tf_op jit(solution)/shard_map/ppermute | solution.py:254
  115.9 4.6 %attend.2 = bf16[8,136,128]{2,1,0:T(8,128)(2,1)} custom-call(bf16[1024,128]{1,0:T(8,128)(2,1)S(1)} %bitcast.46, bf16[1024,256]{1,0:T(8,128)(2,1)S(1)} %fusion.refs_0_, bf16[1024,256]{1,0:T(8,128)(2,1)S(1)} %collective-permute-done.refs_1_), custom_call_target="tpu_custom_call" | custom-call | flops 1073741824 | bytes 1572864 | tf_op jit(solution)/shard_map/attend/pallas_call | solution.py:83
  120.5 8.1 %all-to-all-start.2 = ((bf16[8,136,128]{2,1,0:T(8,128)(2,1)}), bf16[8,136,128]{2,1,0:T(8,128)(2,1)S(1)}, u32[]{:S(2)}, u32[]{:S(2)}) async-start(bf16[8,136,128]{2,1,0:T(8,128)(2,1)} %attend.2), calls=%async_computation.2 | async-start | bytes 557056 | tf_op jit(solution)/shard_map/all_to_all | solution.py:221
  128.6 4.6 %fusion.1.refs_0_ = bf16[1024,256]{1,0:T(8,128)(2,1)} fusion(bf16[1024,2048]{1,0:T(8,128)(2,1)} %all-gather.9.cloned.1.call-done, bf16[2048,128]{1,0:T(8,128)(2,1)} %get-tuple-element.19, bf16[2048,128]{1,0:T(8,128)(2,1)} %get-tuple-element.26), kind=kOutput, calls=%fused_computation.3 | convolution fusion | flops 1076101120 | bytes 5767168 | tf_op jit(solution)/shard_map/dot_general | solution.py:217
  133.2 12.3 %all-to-all-done.2.g_ref = bf16[8,136,128]{2,1,0:T(8,128)(2,1)S(1)} async-done(((bf16[8,136,128]{2,1,0:T(8,128)(2,1)}), bf16[8,136,128]{2,1,0:T(8,128)(2,1)S(1)}, u32[]{:S(2)}, u32[]{:S(2)}) %all-to-all-start.2) | async-done | bytes 278560 | tf_op jit(solution)/shard_map/all_to_all | solution.py:221
  146.2 1.8 join.2
  148.0 4.1 %all-to-all-start.3 = ((bf16[8,128,128]{2,1,0:T(8,128)(2,1)}), bf16[8,128,128]{2,1,0:T(8,128)(2,1)S(1)}, u32[]{:S(2)}, u32[]{:S(2)}) async-start(bf16[8,128,128]{2,1,0:T(8,128)(2,1)} %join.2), calls=%async_computation.3 | async-start | bytes 524288 | tf_op jit(solution)/shard_map/all_to_all | solution.py:221
  152.1 1.9 collective-permute-start.3
  154.1 3.4 %collective-permute-start.2 = (bf16[1024,256]{1,0:T(8,128)(2,1)}, bf16[1024,256]{1,0:T(8,128)(2,1)}, u32[]{:S(2)}, u32[]{:S(2)}) collective-permute-start(bf16[1024,256]{1,0:T(8,128)(2,1)} %fusion.1.refs_0_), channel_id=1, source_target_pairs={{0,16},{16,32},{32,48},{48,64},{64,80},{80,96},{96,112},{112,128},... | collective-permute-start | bytes 1572872 | tf_op jit(solution)/shard_map/ppermute | solution.py:213
  157.5 4.0 %all-to-all-done.3 = bf16[8,128,128]{2,1,0:T(8,128)(2,1)S(1)} async-done(((bf16[8,128,128]{2,1,0:T(8,128)(2,1)}), bf16[8,128,128]{2,1,0:T(8,128)(2,1)S(1)}, u32[]{:S(2)}, u32[]{:S(2)}) %all-to-all-start.3) | async-done | bytes 262176 | tf_op jit(solution)/shard_map/all_to_all | solution.py:221
  161.5 9.0 %all-gather.1 = bf16[16,128,128]{2,1,0:T(8,128)(2,1)S(1)} all-gather(bf16[8,128,128]{2,1,0:T(8,128)(2,1)S(1)} %all-to-all-done.3), channel_id=3, replica_groups=mesh['grp'=2,'far'=4,'mid'=2,'near'=2,'x'=8,'c'=2] {'c'}, dimensions={0}, use_global_device_ids=true | all-gather | bytes 786432 | tf_op jit(solution)/shard_map/all_gather | solution.py:263
  170.4 2.2 copy-done
  173.4 2.1 collective-permute-start.4
  175.5 2.2 all-gather.3
  179.1 6.8 %all-to-all-start.4 = ((bf16[4,128,128]{2,1,0:T(8,128)(2,1)}), bf16[4,128,128]{2,1,0:T(8,128)(2,1)S(1)}, u32[]{:S(2)}, u32[]{:S(2)}) async-start(bf16[4,128,128]{2,1,0:T(8,128)(2,1)} %get-tuple-element.11), calls=%async_computation.4 | async-start | bytes 262144 | tf_op jit(solution)/shard_map/all_to_all | solution.py:221
  185.9 12.3 %all-to-all-done.4 = bf16[4,128,128]{2,1,0:T(8,128)(2,1)S(1)} async-done(((bf16[4,128,128]{2,1,0:T(8,128)(2,1)}), bf16[4,128,128]{2,1,0:T(8,128)(2,1)S(1)}, u32[]{:S(2)}, u32[]{:S(2)}) %all-to-all-start.4) | async-done | bytes 131104 | tf_op jit(solution)/shard_map/all_to_all | solution.py:221
  198.2 5.6 %attend.3 = bf16[4,136,128]{2,1,0:T(8,128)(2,1)} custom-call(bf16[512,128]{1,0:T(8,128)(2,1)S(1)} %bitcast.48, bf16[1024,256]{1,0:T(8,128)(2,1)} %fusion.1.refs_0_, bf16[1024,256]{1,0:T(8,128)(2,1)} %collective-permute-done.2.refs_1_, bf16[1024,256]{1,0:T(8,128)(2,1)} %collective-permute-done.3.refs_2_, bf16[1024,256]{1,0:T(8,128)(2,1)S(1)} %collective-permute-done.4.refs_3_), custom_call_target="tpu_custom_call" | custom-call | flops 1073741824 | bytes 2359296 | tf_op jit(solution)/shard_map/attend/pallas_call | solution.py:83
  203.8 3.8 %all-to-all-start.5 = ((bf16[4,136,128]{2,1,0:T(8,128)(2,1)}), bf16[4,136,128]{2,1,0:T(8,128)(2,1)S(1)}, u32[]{:S(2)}, u32[]{:S(2)}) async-start(bf16[4,136,128]{2,1,0:T(8,128)(2,1)} %attend.3), calls=%async_computation.5 | async-start | bytes 278528 | tf_op jit(solution)/shard_map/all_to_all | solution.py:221
  208.6 11.7 %all-to-all-done.5.g_ref = bf16[4,136,128]{2,1,0:T(8,128)(2,1)S(1)} async-done(((bf16[4,136,128]{2,1,0:T(8,128)(2,1)}), bf16[4,136,128]{2,1,0:T(8,128)(2,1)S(1)}, u32[]{:S(2)}, u32[]{:S(2)}) %all-to-all-start.5) | async-done | bytes 139296 | tf_op jit(solution)/shard_map/all_to_all | solution.py:221
  220.9 1.7 join.3
  222.6 7.8 %all-gather.4 = bf16[2,128,128]{2,1,0:T(8,128)(2,1)S(1)} all-gather(bf16[1,128,128]{2,1,0:T(8,128)(2,1)} %join.3), channel_id=6, replica_groups=mesh['grp'=2,'far'=4,'mid'=2,'near'=2,'x'=8,'c'=2] {'c'}, dimensions={0}, use_global_device_ids=true | all-gather | bytes 98304 | tf_op jit(solution)/shard_map/all_gather | solution.py:266
  231.3 3.6 %all-to-all-start.6 = ((bf16[8,2,8,1024]{3,2,1,0:T(8,128)(2,1)}), bf16[8,2,8,1024]{3,2,1,0:T(8,128)(2,1)S(1)}, u32[]{:S(2)}, u32[]{:S(2)}) async-start(bf16[8,2,8,1024]{3,2,1,0:T(8,128)(2,1)} %mix.3), calls=%async_computation.6 | async-start | bytes 524288 | tf_op jit(solution)/shard_map/all_to_all | solution.py:221
  235.0 12.1 %all-to-all-done.6 = bf16[8,2,8,1024]{3,2,1,0:T(8,128)(2,1)S(1)} async-done(((bf16[8,2,8,1024]{3,2,1,0:T(8,128)(2,1)}), bf16[8,2,8,1024]{3,2,1,0:T(8,128)(2,1)S(1)}, u32[]{:S(2)}, u32[]{:S(2)}) %all-to-all-start.6) | async-done | bytes 262176 | tf_op jit(solution)/shard_map/all_to_all | solution.py:221
  247.0 2.1 all-gather.5
  (43 shorter events, 16.0 us)
Async XLA Ops:
  6.5 49.9 %copy-start.8 = (bf16[8,2048]{1,0:T(8,128)(2,1)S(1)}, bf16[8,2048]{1,0:T(8,128)(2,1)}, u32[]{:S(2)}) copy-start(bf16[8,2048]{1,0:T(8,128)(2,1)} %param.7) | copy-start | bytes 98308
  6.5 54.3 %copy-start.4 = (bf16[2,2048,128]{2,1,0:T(8,128)(2,1)S(1)}, bf16[2,2048,128]{2,1,0:T(8,128)(2,1)}, u32[]{:S(2)}) copy-start(bf16[2,2048,128]{2,1,0:T(8,128)(2,1)} %param.11) | copy-start | bytes 3145732
  6.6 54.3 %copy-start.5 = (bf16[2,2048,128]{2,1,0:T(8,128)(2,1)S(1)}, bf16[2,2048,128]{2,1,0:T(8,128)(2,1)}, u32[]{:S(2)}) copy-start(bf16[2,2048,128]{2,1,0:T(8,128)(2,1)} %param.10) | copy-start | bytes 3145732
  6.6 90.4 %all-gather.9.cloned.1.call-start = ((), (), s32[]{:S(2)}) async-start(), calls=%async_computation.7 | async-start | bytes 4456448 | tf_op jit(solution)/shard_map/all_gather | solution.py:232
  7.3 163.1 %all-gather.11.cloned.1.call-start = ((), (), s32[]{:S(2)}) async-start(), calls=%async_computation.8 | async-start | bytes 4718592 | tf_op jit(solution)/shard_map/all_gather | solution.py:262
  8.5 44.9 %collective-permute-start.1 = (bf16[2,128,1024]{2,1,0:T(8,128)(2,1)S(1)}, bf16[2,128,1024]{2,1,0:T(8,128)(2,1)S(1)}, u32[]{:S(2)}, u32[]{:S(2)}) collective-permute-start(bf16[2,128,1024]{2,1,0:T(8,128)(2,1)S(1)} %constant_dynamic-slice_fusion.1), channel_id=1, source_target_pairs={{0,1},{1,0},{2,3},{3,2},{4,5},{5,4},{6,7},{7,6},{8,9},{9,8},{10,11... | collective-permute-start | bytes 1572872 | tf_op jit(solution)/shard_map/ppermute | solution.py:240
  55.5 22.5 %copy-start.1 = (bf16[2,2048,128]{2,1,0:T(8,128)(2,1)S(1)}, bf16[2,2048,128]{2,1,0:T(8,128)(2,1)}, u32[]{:S(2)}) copy-start(bf16[2,2048,128]{2,1,0:T(8,128)(2,1)} %w_ref.3) | copy-start | bytes 3145732
  55.5 22.5 %copy-start.2 = (f32[2,2,2048]{2,1,0:T(2,128)S(1)}, f32[2,2,2048]{2,1,0:T(2,128)}, u32[]{:S(2)}) copy-start(f32[2,2,2048]{2,1,0:T(2,128)} %gains_ref.3) | copy-start | bytes 98308
  57.2 18.2 %all-to-all-start = ((bf16[8,8,2048]{2,1,0:T(8,128)(2,1)}), bf16[8,8,2048]{2,1,0:T(8,128)(2,1)S(1)}, u32[]{:S(2)}, u32[]{:S(2)}) async-start(bf16[8,8,2048]{2,1,0:T(8,128)(2,1)} %broadcast_in_dim.4), calls=%async_computation | async-start | bytes 524288 | tf_op jit(solution)/shard_map/all_to_all | solution.py:221
  79.2 23.4 %all-to-all-start.1 = ((bf16[8,128,128]{2,1,0:T(8,128)(2,1)}), bf16[8,128,128]{2,1,0:T(8,128)(2,1)S(1)}, u32[]{:S(2)}, u32[]{:S(2)}) async-start(bf16[8,128,128]{2,1,0:T(8,128)(2,1)} %query.2), calls=%async_computation.1 | async-start | bytes 524288 | tf_op jit(solution)/shard_map/all_to_all | solution.py:221
  100.7 15.2 %collective-permute-start = (bf16[1024,256]{1,0:T(8,128)(2,1)S(1)}, bf16[1024,256]{1,0:T(8,128)(2,1)S(1)}, u32[]{:S(2)}, u32[]{:S(2)}) collective-permute-start(bf16[1024,256]{1,0:T(8,128)(2,1)S(1)} %fusion.refs_0_), channel_id=1, source_target_pairs={{0,16},{16,0},{1,17},{17,1},{2,18},{18,2},{3,19},{19,3},{4,20},{20... | collective-permute-start | bytes 1572872 | tf_op jit(solution)/shard_map/ppermute | solution.py:254
  120.5 25.0 %all-to-all-start.2 = ((bf16[8,136,128]{2,1,0:T(8,128)(2,1)}), bf16[8,136,128]{2,1,0:T(8,128)(2,1)S(1)}, u32[]{:S(2)}, u32[]{:S(2)}) async-start(bf16[8,136,128]{2,1,0:T(8,128)(2,1)} %attend.2), calls=%async_computation.2 | async-start | bytes 557056 | tf_op jit(solution)/shard_map/all_to_all | solution.py:221
  145.5 0.7 copy-start.3
  148.0 13.4 %all-to-all-start.3 = ((bf16[8,128,128]{2,1,0:T(8,128)(2,1)}), bf16[8,128,128]{2,1,0:T(8,128)(2,1)S(1)}, u32[]{:S(2)}, u32[]{:S(2)}) async-start(bf16[8,128,128]{2,1,0:T(8,128)(2,1)} %join.2), calls=%async_computation.3 | async-start | bytes 524288 | tf_op jit(solution)/shard_map/all_to_all | solution.py:221
  152.1 21.2 %collective-permute-start.3 = (bf16[1024,256]{1,0:T(8,128)(2,1)}, bf16[1024,256]{1,0:T(8,128)(2,1)}, u32[]{:S(2)}, u32[]{:S(2)}) collective-permute-start(bf16[1024,256]{1,0:T(8,128)(2,1)} %fusion.1.refs_0_), channel_id=1, source_target_pairs={{0,240},{16,0},{32,16},{48,32},{64,48},{80,64},{96,80},{112,96},{1... | collective-permute-start | bytes 1572872 | tf_op jit(solution)/shard_map/ppermute | solution.py:213
  154.1 31.8 %collective-permute-start.2 = (bf16[1024,256]{1,0:T(8,128)(2,1)}, bf16[1024,256]{1,0:T(8,128)(2,1)}, u32[]{:S(2)}, u32[]{:S(2)}) collective-permute-start(bf16[1024,256]{1,0:T(8,128)(2,1)} %fusion.1.refs_0_), channel_id=1, source_target_pairs={{0,16},{16,32},{32,48},{48,64},{64,80},{80,96},{96,112},{112,128},... | collective-permute-start | bytes 1572872 | tf_op jit(solution)/shard_map/ppermute | solution.py:213
  170.4 2.2 copy-start
  173.4 34.3 %copy-start.6 = (bf16[128,1024]{1,0:T(8,128)(2,1)S(1)}, bf16[128,1024]{1,0:T(8,128)(2,1)}, u32[]{:S(2)}) copy-start(bf16[128,1024]{1,0:T(8,128)(2,1)} %get-tuple-element.23) | copy-start | bytes 786436
  173.4 24.8 %collective-permute-start.4 = (bf16[1024,256]{1,0:T(8,128)(2,1)}, bf16[1024,256]{1,0:T(8,128)(2,1)S(1)}, u32[]{:S(2)}, u32[]{:S(2)}) collective-permute-start(bf16[1024,256]{1,0:T(8,128)(2,1)} %collective-permute-done.3.refs_2_), channel_id=1, source_target_pairs={{0,240},{16,0},{32,16},{48,32},{64,48},{80,64},{96,80},{112,96},{1... | collective-permute-start | bytes 1572872 | tf_op jit(solution)/shard_map/ppermute | solution.py:213
  179.1 19.1 %all-to-all-start.4 = ((bf16[4,128,128]{2,1,0:T(8,128)(2,1)}), bf16[4,128,128]{2,1,0:T(8,128)(2,1)S(1)}, u32[]{:S(2)}, u32[]{:S(2)}) async-start(bf16[4,128,128]{2,1,0:T(8,128)(2,1)} %get-tuple-element.11), calls=%async_computation.4 | async-start | bytes 262144 | tf_op jit(solution)/shard_map/all_to_all | solution.py:221
  203.8 16.5 %all-to-all-start.5 = ((bf16[4,136,128]{2,1,0:T(8,128)(2,1)}), bf16[4,136,128]{2,1,0:T(8,128)(2,1)S(1)}, u32[]{:S(2)}, u32[]{:S(2)}) async-start(bf16[4,136,128]{2,1,0:T(8,128)(2,1)} %attend.3), calls=%async_computation.5 | async-start | bytes 278528 | tf_op jit(solution)/shard_map/all_to_all | solution.py:221
  220.3 0.7 copy-start.7
  231.3 15.7 %all-to-all-start.6 = ((bf16[8,2,8,1024]{3,2,1,0:T(8,128)(2,1)}), bf16[8,2,8,1024]{3,2,1,0:T(8,128)(2,1)S(1)}, u32[]{:S(2)}, u32[]{:S(2)}) async-start(bf16[8,2,8,1024]{3,2,1,0:T(8,128)(2,1)} %mix.3), calls=%async_computation.6 | async-start | bytes 524288 | tf_op jit(solution)/shard_map/all_to_all | solution.py:221
Sparse Core Ops, SparseCore 0:
  9.5 87.4 all-gather.8
  99.1 54.8 all-gather.10
